TPU v7x, 128 devices: a whole 4x4x4 slice. The times are simulated.
128 devices in a mesh: kv: 16 (over z, x), tp: 8 (over y, core).
Axes of the slice: x: 4, y: 4, z: 4, core: 2. Of those that a mesh axis runs over, the one named last changes fastest.
Arguments:
- tokens: bfloat16 [32768, 2048], P('kv'), may hold values from -6 to 6
- norm_gain: bfloat16 [2048], replicated, may hold values from 0.099609375 to 1.8984375
- query_weight: bfloat16 [2048, 1024], P(None, 'tp'), may hold values from -0.125 to 0.125
- cmp_key_weight: bfloat16 [2048, 512], P(None, 'tp'), may hold values from -0.125 to 0.125
- cmp_value_weight: bfloat16 [2048, 512], P(None, 'tp'), may hold values from -0.125 to 0.125
- sel_key_weight: bfloat16 [2048, 512], P(None, 'tp'), may hold values from -0.125 to 0.125
- sel_value_weight: bfloat16 [2048, 512], P(None, 'tp'), may hold values from -0.125 to 0.125
- branch_weight: bfloat16 [2, 2048, 16], replicated, may hold values from -0.125 to 0.125
- key_embed: bfloat16 [8, 32, 64], P('tp'), may hold values from -3 to 3
- key_inner: bfloat16 [8, 2048, 64], P('tp'), may hold values from -0.125 to 0.125
- key_outer: bfloat16 [8, 64, 64], P('tp'), may hold values from -0.75 to 0.75
- value_embed: bfloat16 [8, 32, 64], P('tp'), may hold values from -3 to 3
- value_inner: bfloat16 [8, 2048, 64], P('tp'), may hold values from -0.125 to 0.125
- value_outer: bfloat16 [8, 64, 64], P('tp'), may hold values from -0.75 to 0.75
- out_weight: bfloat16 [1024, 2048], replicated, may hold values from -0.1875 to 0.1875
- chosen: int32 [8, 256, 8], P('tp'), may hold values from 0 to 511, as said below
Outputs:
- attended: bfloat16 [32768, 2048], P(('kv', 'tp'))
Inputs may be any that keep to these rules, and one draw needn't show every extreme that they name: `chosen`: each entry is the index of a block of 64 positions in the whole sequence. For every key head and query block, its 8 entries lie in 8 different aligned spans of 2048 positions (at most one from any span), and none lies inside the query block's own positions.
All inputs are finite; a program needn't handle non-finite values.
Results may differ from a plain program's by a relative error of at most 0.0075.
Values may be sent and summed in bfloat16 or wider, within the bound.
A program may use at most 128 MiB of HBM per device.

v0:
```python
import functools

import jax
import jax.numpy as jnp
from jax import lax
from jax.experimental import pallas as pl
from jax.experimental.pallas import tpu as pltpu
from jax.sharding import PartitionSpec as P

HEAD_DIM = 64
CMP_BLOCK = 32
SEL_BLOCK = 64
Q_BLOCK = 128
FAR_PICKS = 8
LANES = 2 * HEAD_DIM
PLANES = 4
MESH = pl.DeviceIdType.MESH

ROPE_BASE = 10000.0
norm_eps = 1e-06
MASKED = -1e30

def params(n_axes, limit=48):
    return pltpu.CompilerParams(
        dimension_semantics=("arbitrary",) * n_axes, vmem_limit_bytes=limit * 1024 * 1024
    )


def norm_rows(tok_ref, gain_ref):
    x = tok_ref[...].astype(jnp.float32)
    inv = lax.rsqrt(jnp.mean(x * x, axis=-1, keepdims=True) + norm_eps)
    return (x * inv * gain_ref[...].astype(jnp.float32)).astype(jnp.bfloat16)


def turn(x, cosine, sine_up, sine_down):
    quarter = HEAD_DIM // 2
    return (
        x * cosine
        + pltpu.roll(x, LANES - quarter, 1) * sine_up
        + pltpu.roll(x, quarter, 1) * sine_down
    )


def low_lanes(shape):
    return lax.broadcasted_iota(jnp.int32, shape, 1) < HEAD_DIM


def sel_kernel(tok_ref, gain_ref, w_ref, cos_ref, up_ref, down_ref, *outs):
    normed = norm_rows(tok_ref, gain_ref)
    y = jnp.dot(normed, w_ref[...], preferred_element_type=jnp.float32)
    for k, out in enumerate(outs):
        x = y[:, k * LANES : (k + 1) * LANES]
        low = low_lanes(x.shape)
        turned = turn(x, cos_ref[...], up_ref[...], down_ref[...])
        out[...] = jnp.where(low, turned, x).astype(jnp.bfloat16)


def nt_dot(a, b):
    return lax.dot_general(a, b, (((1,), (1,)), ((), ())), preferred_element_type=jnp.float32)


def gate_lanes(gate, first, shape):
    return jnp.where(low_lanes(shape), gate[:, first : first + 1], gate[:, first + 1 : first + 2])


def merge(out, rows):
    low = low_lanes((rows, LANES))
    return jnp.where(low, pltpu.roll(out[:rows], HEAD_DIM, 1), out[rows:])


def exchange_kernel(
    planes,
    idx_ref,
    bias_ref,
    gain_ref,
    ke_ref,
    ko_ref,
    ve_ref,
    vo_ref,
    tok_hbm,
    w_hbm,
    cos_hbm,
    up_hbm,
    down_hbm,
    ki_hbm,
    vi_hbm,
    *rest,
):
    kv_local = bias_ref.shape[0]
    own_hbm, rest = rest[:kv_local], rest[kv_local:]
    out_ref, rest = rest[0], rest[1:]
    held, rest = rest[:kv_local], rest[kv_local:]
    (
        tok,
        w,
        cosine,
        up,
        down,
        ki,
        vi,
        qp,
        qt,
        ck,
        cv,
        gate,
        sums,
        oc,
        mix,
        got,
        local_sem,
        send_sem,
        recv_sem,
        sum_send,
        sum_recv,
        mix_send,
        mix_recv,
    ) = rest
    owners, ranks = sums.shape[0], got.shape[0]
    rows, width = tok.shape
    span = rows // SEL_BLOCK
    across = owners // planes
    me, rank = lax.axis_index("kv"), lax.axis_index("tp")
    z, x = me // across, me % across

    barrier = pltpu.get_barrier_semaphore()
    for d in range(1, owners):
        pl.semaphore_signal(barrier, inc=1, device_id={"kv": (me + d) % owners}, device_id_type=MESH)
    for d in range(1, ranks):
        pl.semaphore_signal(barrier, inc=1, device_id={"tp": (rank + d) % ranks}, device_id_type=MESH)
    loads = [
        (tok_hbm, tok),
        (w_hbm, w),
        (cos_hbm, cosine),
        (up_hbm, up),
        (down_hbm, down),
        (ki_hbm, ki),
        (vi_hbm, vi),
    ]
    copies = [pltpu.make_async_copy(a, b, local_sem.at[n]) for n, (a, b) in enumerate(loads)]
    for k in range(kv_local):
        copies.append(
            pltpu.make_async_copy(own_hbm[k], held[k].at[pl.ds(0, span)], local_sem.at[len(loads) + k])
        )
    for copy in copies:
        copy.start()
    pl.semaphore_wait(barrier, owners + ranks - 2)

    def slot(k, n):
        return held[k].at[pl.ds(n * span, span)]

    def hop(k, dz, dx):
        n = dz * across + dx
        if dx:
            source = own_hbm[k] if dz == 0 else slot(k, dz * across)
            target = z * across + (x + dx) % across
            sends = (x + dx < across) if dz == 0 else (z >= dz)
            gets = (x >= dx) if dz == 0 else (z >= dz)
        else:
            step = 1 if dz == 3 else dz
            source = slot(k, 2 * across) if dz == 3 else own_hbm[k]
            target = lax.rem(me + step * across, owners)
            sends = (z == 2) if dz == 3 else (z + dz < planes)
            gets = z >= dz
        copy = pltpu.make_async_remote_copy(
            src_ref=source,
            dst_ref=slot(k, n),
            send_sem=send_sem.at[k, n],
            recv_sem=recv_sem.at[k, n],
            device_id={"kv": target},
            device_id_type=MESH,
        )
        return copy, sends, gets

    def send(k, dz, dx):
        copy, sends, _ = hop(k, dz, dx)
        pl.when(sends)(copy.start)

    def arrive(k, dz, dx):
        copy, _, gets = hop(k, dz, dx)
        pl.when(gets)(copy.wait_recv)

    def send_own(k):
        for dz in (2, 1):
            if dz < planes:
                send(k, dz, 0)
        for dx in range(1, across):
            send(k, 0, dx)

    def forward(k, dz):
        if dz >= planes:
            return
        arrive(k, dz, 0)
        if dz == 2 and planes > 3:
            send(k, 3, 0)
        for dx in range(1, across):
            send(k, dz, dx)

    send_own(0)
    for copy in copies:
        copy.wait()

    tile = 256
    scale = HEAD_DIM ** (-0.5)
    base = kv_local * LANES
    kv_width = kv_local * HEAD_DIM

    def project(i, carry):
        at = pl.ds(pl.multiple_of(i * tile, tile), tile)
        normed = norm_rows(tok.at[at], gain_ref)
        y = jnp.dot(normed, w[...], preferred_element_type=jnp.float32)
        for k in range(kv_local):
            v = y[:, k * LANES : (k + 1) * LANES]
            low = low_lanes(v.shape)
            turned = turn(v, cosine[at], up[at], down[at]) * scale
            for ref, q in ((qp, v * scale), (qt, turned)):
                ref[k, 0, at] = jnp.where(low, q, 0.0).astype(jnp.bfloat16)
                ref[k, 1, at] = jnp.where(low, pltpu.roll(q, HEAD_DIM, 1), 0.0).astype(jnp.bfloat16)
        ck[at] = y[:, base : base + kv_width].astype(jnp.bfloat16).astype(jnp.float32)
        cv[at] = y[:, base + kv_width : base + 2 * kv_width].astype(jnp.bfloat16).astype(jnp.float32)
        gate[at] = jax.nn.sigmoid(y[:, base + 2 * kv_width :])
        return carry

    lax.fori_loop(0, rows // tile, project, 0)

    blocks = rows // CMP_BLOCK

    def summarize(x_ref, e_ref, i_ref, o_ref):
        parts = []
        for c in range(CMP_BLOCK):
            part = x_ref[pl.ds(c, blocks, stride=CMP_BLOCK), :] + e_ref[c : c + 1, :]
            parts.append(part.astype(jnp.bfloat16))
        flat = jnp.concatenate(parts, axis=1)
        hidden = jnp.dot(flat, i_ref[...], preferred_element_type=jnp.float32)
        hidden = jax.nn.gelu(hidden).astype(jnp.bfloat16)
        return jnp.dot(hidden, o_ref[...], preferred_element_type=jnp.float32)

    sk = summarize(ck, ke_ref, ki, ko_ref)
    sv = summarize(cv, ve_ref, vi, vo_ref)
    for k in range(kv_local):
        cut = slice(k * HEAD_DIM, (k + 1) * HEAD_DIM)
        sums[me, k] = jnp.concatenate([sk[:, cut], sv[:, cut]], axis=1).astype(jnp.bfloat16)

    def sum_copy(d, source):
        return pltpu.make_async_remote_copy(
            src_ref=sums.at[source],
            dst_ref=sums.at[source],
            send_sem=sum_send.at[d],
            recv_sem=sum_recv.at[d],
            device_id={"kv": (me + d) % owners},
            device_id_type=MESH,
        )

    for d in range(1, owners):
        sum_copy(d, me).start()
    for k in range(1, kv_local):
        send_own(k)
    forward(0, 2)
    forward(0, 1)
    for d in range(1, owners):
        sum_copy(d, (me + owners - d) % owners).wait_recv()

    def compress(i, carry):
        at = pl.ds(pl.multiple_of(i * tile, tile), tile)
        row = lax.broadcasted_iota(jnp.int32, (2 * tile, 1), 0)
        pos = me * rows + i * tile + jnp.where(row >= tile, row - tile, row)
        lane = lax.broadcasted_iota(jnp.int32, (1, owners * blocks), 1)
        allowed = (lane + 1) * CMP_BLOCK - 1 <= pos
        for k in range(kv_local):
            keys = jnp.concatenate([sums[s, k] for s in range(owners)], axis=0)
            q = jnp.concatenate([qp[k, 0, at], qp[k, 1, at]], axis=0)
            s = jnp.where(allowed, nt_dot(q, keys), MASKED)
            top = jnp.max(s, axis=-1, keepdims=True)
            e = jnp.where(allowed, jnp.exp(s - top), 0.0)
            total = jnp.sum(e, axis=-1, keepdims=True)
            o = jnp.dot(e.astype(jnp.bfloat16), keys, preferred_element_type=jnp.float32)
            o = o * jnp.where(total > 0.0, 1.0 / jnp.where(total > 0.0, total, 1.0), 0.0)
            o = merge(o, tile)
            oc[k, at] = o * gate_lanes(gate[at], 2 * k, o.shape)
        return carry

    lax.fori_loop(0, rows // tile, compress, 0)

    rank_rows = rows // ranks
    group = rank_rows // Q_BLOCK
    q_blocks = rows // Q_BLOCK
    half_gates = 2 * kv_local

    def mix_copy(k, step):
        target = (rank + 1 + step) % ranks
        at = pl.ds(pl.multiple_of(target * rank_rows, rank_rows), rank_rows)
        return pltpu.make_async_remote_copy(
            src_ref=mix.at[k, at],
            dst_ref=got.at[rank, k],
            send_sem=mix_send.at[k, step],
            recv_sem=mix_recv.at[k, step],
            device_id={"tp": target},
            device_id_type=MESH,
        )

    def choose(k):
        def one(step, carry):
            target = (rank + 1 + step) % ranks
            for u in range(group):
                j = target * group + u
                at = pl.ds(pl.multiple_of(j * Q_BLOCK, Q_BLOCK), Q_BLOCK)
                own = j * (Q_BLOCK // SEL_BLOCK)
                parts = [held[k][own + b] for b in range(Q_BLOCK // SEL_BLOCK)]
                for a in range(FAR_PICKS):
                    pick = idx_ref[(k * q_blocks + j) * FAR_PICKS + a]
                    parts.append(held[k][pick])
                keys = jnp.concatenate(parts, axis=0)
                q = jnp.concatenate([qt[k, 0, at], qt[k, 1, at]], axis=0)
                s = nt_dot(q, keys) + bias_ref[k, j]
                row = lax.broadcasted_iota(jnp.int32, (2 * Q_BLOCK, Q_BLOCK), 0)
                row = jnp.where(row >= Q_BLOCK, row - Q_BLOCK, row)
                lane = lax.broadcasted_iota(jnp.int32, row.shape, 1)
                near = jnp.where(lane > row, MASKED, s[:, :Q_BLOCK])
                s = jnp.concatenate([near, s[:, Q_BLOCK:]], axis=1)
                top = jnp.max(s, axis=-1, keepdims=True)
                e = jnp.exp(s - top)
                total = jnp.sum(e, axis=-1, keepdims=True)
                o = jnp.dot(e.astype(jnp.bfloat16), keys, preferred_element_type=jnp.float32)
                o = merge(o * (1.0 / total), Q_BLOCK)
                g = gate_lanes(gate[at], half_gates + 2 * k, o.shape)
                mix[k, at] = (oc[k, at] + o * g).astype(jnp.bfloat16)
            pl.when(step > 0)(lambda: mix_copy(k, step - 1).start())
            return carry

        lax.fori_loop(0, ranks, one, 0)

    moves = [(dz, dx) for dz in range(planes) for dx in range(across) if (dz, dx) != (0, 0)]
    for k in range(kv_local):
        if k:
            forward(k, 2)
            forward(k, 1)
        forward(k, 3)
        for dz, dx in moves:
            if dx:
                arrive(k, dz, dx)
        choose(k)
    own_at = pl.ds(pl.multiple_of(rank * rank_rows, rank_rows), rank_rows)
    for k in range(kv_local):
        for dz, dx in moves:
            copy, sends, _ = hop(k, dz, dx)
            pl.when(sends)(copy.wait_send)
    for d in range(1, owners):
        sum_copy(d, me).wait_send()
    for k in range(kv_local):
        got[rank, k] = mix[k, own_at]
        for step in range(ranks - 1):
            mix_copy(k, step).wait_send()
            mix_copy(k, step).wait_recv()
    for t in range(ranks):
        for k in range(kv_local):
            first = (t * kv_local + k) * LANES
            out_ref[:, first : first + LANES] = got[t, k]


def cost(flops, moved):
    return pl.CostEstimate(flops=int(flops), bytes_accessed=int(moved), transcendentals=0)


def block_diagonal(w):
    n, a, b = w.shape
    zero = jnp.zeros((a, b), w.dtype)
    return jnp.concatenate(
        [jnp.concatenate([w[i] if i == j else zero for j in range(n)], axis=1) for i in range(n)],
        axis=0,
    )


def inner_diagonal(w):
    n, rows, e = w.shape
    w = w.reshape(n, CMP_BLOCK, HEAD_DIM, e)
    zero = jnp.zeros_like(w[0])
    full = jnp.stack(
        [jnp.concatenate([w[i] if i == j else zero for j in range(n)], axis=-1) for i in range(n)],
        axis=1,
    )
    return full.reshape(CMP_BLOCK * n * HEAD_DIM, n * e)


def per_device(
    tokens,
    norm_gain,
    query_weight,
    cmp_key_weight,
    cmp_value_weight,
    sel_key_weight,
    sel_value_weight,
    branch_weight,
    key_embed,
    key_inner,
    key_outer,
    value_embed,
    value_inner,
    value_outer,
    out_weight,
    chosen,
):
    rows, width = tokens.shape
    kv_local = key_embed.shape[0]
    heads_local = query_weight.shape[1] // HEAD_DIM
    owners = lax.axis_size("kv")
    me = lax.axis_index("kv")
    planes = PLANES if owners % PLANES == 0 else 1
    across = owners // planes
    my_z, my_x = me // across, me % across
    offset = me * rows
    f32 = jnp.float32
    bf16 = jnp.bfloat16

    half = HEAD_DIM // 2
    lane = jnp.arange(LANES, dtype=jnp.int32)
    inverse = ROPE_BASE ** (-(lane % half).astype(f32) / half)
    positions = offset + jnp.arange(rows, dtype=jnp.int32)
    phases = positions.astype(f32)[:, None] * inverse[None, :]
    cosine = jnp.cos(phases)
    sine = jnp.sin(phases)
    first = (lane % HEAD_DIM < half)[None, :]
    up = jnp.where(first, -sine, 0.0)
    down = jnp.where(first, 0.0, sine)
    gain = norm_gain.reshape(1, width)

    def heads_of(w, k):
        return w[:, k * HEAD_DIM : (k + 1) * HEAD_DIM]

    sel_weight = jnp.concatenate(
        [heads_of(w, k) for k in range(kv_local) for w in (sel_key_weight, sel_value_weight)],
        axis=1,
    )
    tile = 256
    steps = rows // tile
    row_spec = lambda cols: pl.BlockSpec((tile, cols), lambda i: (i, 0))
    full = lambda shape: pl.BlockSpec(shape, lambda *_: (0,) * len(shape))
    kv = pl.pallas_call(
        sel_kernel,
        grid=(steps,),
        in_specs=[row_spec(width), full((1, width)), full(sel_weight.shape)]
        + [row_spec(LANES)] * 3,
        out_specs=[row_spec(LANES)] * kv_local,
        out_shape=[jax.ShapeDtypeStruct((rows, LANES), bf16)] * kv_local,
        compiler_params=params(1),
        cost_estimate=cost(2 * rows * width * sel_weight.shape[1], rows * width * 2),
        name="sel_project",
    )(tokens, gain, sel_weight, cosine, up, down)

    gate_cols = lax.dynamic_slice_in_dim(
        branch_weight, lax.axis_index("tp") * heads_local, heads_local, 2
    )
    gate_weight = jnp.concatenate([gate_cols[0], gate_cols[1]], axis=1)
    gate_count = 2 * heads_local
    mid_weight = jnp.concatenate(
        [query_weight, cmp_key_weight, cmp_value_weight, jnp.pad(gate_weight, ((0, 0), (0, LANES - gate_count)))],
        axis=1,
    )
    kv_width = kv_local * HEAD_DIM
    blocks = rows // CMP_BLOCK
    embeds = [
        e.astype(f32).transpose(1, 0, 2).reshape(CMP_BLOCK, kv_width)
        for e in (key_embed, value_embed)
    ]
    q_blocks = rows // Q_BLOCK
    span_blocks = rows // SEL_BLOCK
    picks = lax.dynamic_slice_in_dim(chosen.astype(jnp.int32), me * q_blocks, q_blocks, 1)
    own_first = (me * q_blocks + jnp.arange(q_blocks, dtype=jnp.int32)) * (Q_BLOCK // SEL_BLOCK)
    usable = picks < own_first[None, :, None]
    span = picks // span_blocks
    slot = (my_z - span // across) * across + (my_x - span % across) % across
    index = jnp.where(usable, slot * span_blocks + picks % span_blocks, 0).reshape(-1)
    bias = jnp.where(usable, 0.0, MASKED).astype(f32)
    bias = jnp.repeat(bias, SEL_BLOCK, axis=-1)
    bias = jnp.pad(bias, ((0, 0), (0, 0), (Q_BLOCK, 0)))[:, :, None, :]

    ranks = lax.axis_size("tp")
    rank_rows = rows // ranks
    key_diag, value_diag = inner_diagonal(key_inner), inner_diagonal(value_inner)
    operands = (
        index,
        bias,
        gain,
        embeds[0],
        block_diagonal(key_outer),
        embeds[1],
        block_diagonal(value_outer),
        tokens,
        mid_weight,
        cosine,
        up,
        down,
        key_diag,
        value_diag,
        *[own.reshape(span_blocks, SEL_BLOCK, LANES) for own in kv],
    )
    vmem = pl.BlockSpec(memory_space=pltpu.VMEM)
    hbm = pl.BlockSpec(memory_space=pl.ANY)
    dma = pltpu.SemaphoreType.DMA
    spread = pltpu.VMEM((kv_local, 2, rows, LANES), bf16)
    gathered = pl.pallas_call(
        functools.partial(exchange_kernel, planes),
        in_specs=[pl.BlockSpec(memory_space=pltpu.SMEM)] + [vmem] * 6 + [hbm] * (7 + kv_local),
        out_specs=vmem,
        out_shape=jax.ShapeDtypeStruct((rank_rows, ranks * kv_local * LANES), bf16),
        scratch_shapes=[pltpu.VMEM((owners * span_blocks, SEL_BLOCK, LANES), bf16)] * kv_local
        + [
            pltpu.VMEM(tokens.shape, bf16),
            pltpu.VMEM(mid_weight.shape, bf16),
            pltpu.VMEM(cosine.shape, f32),
            pltpu.VMEM(cosine.shape, f32),
            pltpu.VMEM(cosine.shape, f32),
            pltpu.VMEM(key_diag.shape, bf16),
            pltpu.VMEM(value_diag.shape, bf16),
            spread,
            spread,
            pltpu.VMEM((rows, kv_width), f32),
            pltpu.VMEM((rows, kv_width), f32),
            pltpu.VMEM((rows, LANES), f32),
            pltpu.VMEM((owners, kv_local, blocks, LANES), bf16),
            pltpu.VMEM((kv_local, rows, LANES), f32),
            pltpu.VMEM((kv_local, rows, LANES), bf16),
            pltpu.VMEM((ranks, kv_local, rank_rows, LANES), bf16),
            dma((7 + kv_local,)),
            dma((kv_local, owners)),
            dma((kv_local, owners)),
            dma((owners,)),
            dma((owners,)),
            dma((kv_local, ranks)),
            dma((kv_local, ranks)),
        ],
        compiler_params=pltpu.CompilerParams(
            collective_id=0, has_side_effects=True, vmem_limit_bytes=60 * 1024 * 1024
        ),
        cost_estimate=cost(4e10, 2e7),
        name="exchange",
    )(*operands)
    return jnp.dot(gathered, out_weight, preferred_element_type=f32).astype(bf16)


def solution(mesh):
    placed = (
        P("kv", None),
        P(),
        P(None, "tp"),
        P(None, "tp"),
        P(None, "tp"),
        P(None, "tp"),
        P(None, "tp"),
        P(),
        P("tp", None, None),
        P("tp", None, None),
        P("tp", None, None),
        P("tp", None, None),
        P("tp", None, None),
        P("tp", None, None),
        P(),
        P("tp", None, None),
    )
    return jax.shard_map(
        per_device, mesh=mesh, in_specs=placed, out_specs=P(("kv", "tp"), None), check_vma=False
    )
```

profile of v0, /device:TPU:111, one launch (start us, length us, event | category | flops | bytes accessed | tf_op | source)
XLA Modules:
  0.0 147.0 jit_solution(11993154726359122930)
XLA Ops:
  0.0 0.8 select_bitcast_fusion
  0.8 0.8 fusion.10
  1.6 0.1 copy.35
  1.7 0.7 reshape.49.idx_ref
  2.5 0.7 reshape.50.gain_ref
  3.2 0.8 dynamic-slice_bitcast_fusion.1
  4.0 1.3 bitcast_convert_fusion
  5.3 0.1 broadcast_in_dim.46
  5.4 0.1 broadcast_in_dim.47
  5.5 0.6 pad_bitcast_fusion.bias_ref
  6.1 0.3 copy.37
  6.5 1.3 copy.38
  7.7 1.2 copy.39
  9.0 2.8 %fusion.1.w_hbm = bf16[2048,384]{1,0:T(8,128)(2,1)} fusion(bf16[2048,4]{1,0:T(8,128)(2,1)S(1)} %copy.37, bf16[2048,64]{1,0:T(8,128)(2,1)S(1)} %copy.39, bf16[2048,64]{1,0:T(8,128)(2,1)S(1)} %copy.38, bf16[2048,128]{1,0:T(8,128)(2,1)} %param.18), kind=kLoop, calls=%fused_computation.3 | loop fusion | flops 7864320 | bytes 2637824 | tf_op jit(solution)/shard_map/concatenate | solution.py:453
  11.8 0.3 copy.42
  12.1 0.3 copy.43
  12.4 0.3 pad_maximum_fusion.w_ref
  12.7 1.0 copy.40
  13.7 1.0 copy.41
  14.7 3.8 %fusion.2 = (f32[2048,128]{1,0:T(8,128)S(1)}, f32[2048,128]{1,0:T(8,128)S(1)}, f32[2048,128]{1,0:T(8,128)S(1)}) fusion(f32[128]{0:T(128)S(1)} %fusion.19, f32[2048]{0:T(1024)S(1)} %add_convert_fusion, pred[128]{0:T(512)(128)(4,1)S(1)} %fusion.20), kind=kLoop, calls=%fused_computation.6 | loop fusion | flops 1048576 | bytes 3154560 | tf_op jit(solution)/shard_map/jit(_where)/select_n | solution.py:422
  18.5 10.0 %sel_project.1 = bf16[2048,128]{1,0:T(8,128)(2,1)S(1)} custom-call(bf16[2048,2048]{1,0:T(8,128)(2,1)} %tok_hbm.1, bf16[1,2048]{1,0:T(2,128)(2,1)S(1)} %reshape.50.gain_ref, bf16[2048,128]{1,0:T(8,128)(2,1)S(1)} %pad_maximum_fusion.w_ref, f32[2048,128]{1,0:T(8,128)S(1)} %get-tuple-element.11.cos_ref.cos_hbm, f32[2048,128]{1,0:T(8,128)S(1)} %get-tuple-element.10.up_ref.up_hbm, ...), custom_call_target="tpu_custom_call" | custom-call | flops 1073741824 | bytes 8388608 | tf_op jit(solution)/shard_map/sel_project/pallas_call | solution.py:436
  28.6 0.8 copy-done.3
  29.4 113.1 %exchange.1 = bf16[256,1024]{1,0:T(8,128)(2,1)} custom-call(s32[128]{0:T(128)} %reshape.49.idx_ref, f32[1,16,1,640]{3,2,1,0:T(1,128)} %pad_bitcast_fusion.bias_ref, bf16[1,2048]{1,0:T(2,128)(2,1)} %copy-done.4, f32[32,64]{1,0:T(8,128)} %get-tuple-element.13.ke_ref, bf16[64,64]{1,0:T(8,128)(2,1)} %bitcast.24, f32[32,64]{1,0:T(8,128)} %get-tuple-element.12.ve_ref, ...), custom_call_target="tpu_custom_call" | custom-call | flops 40000000000 | bytes 20000000 | tf_op jit(solution)/shard_map/exchange/pallas_call | solution.py:499
  142.5 4.6 %convolution_convert_fusion = bf16[256,2048]{1,0:T(8,128)(2,1)} fusion(bf16[256,1024]{1,0:T(8,128)(2,1)} %exchange.1, bf16[1024,2048]{1,0:T(8,128)(2,1)} %param.30), kind=kOutput, calls=%fused_computation.2 | convolution fusion | flops 1074266112 | bytes 5767168 | tf_op jit(solution)/shard_map/dot_general | solution.py:536
  (23 shorter events, 0.2 us)
Async XLA Ops:
  0.0 11.8 %copy-start.5 = (bf16[2048,64]{0,1:T(8,128)(2,1)S(1)}, bf16[2048,64]{0,1:T(8,128)(2,1)}, u32[]{:S(2)}) copy-start(bf16[2048,64]{0,1:T(8,128)(2,1)} %param.21) | copy-start | bytes 786436
  3.2 15.4 %copy-start.4 = (bf16[1,2048]{1,0:T(2,128)(2,1)}, bf16[1,2048]{1,0:T(2,128)(2,1)S(1)}, u32[]{:S(2)}) copy-start(bf16[1,2048]{1,0:T(2,128)(2,1)S(1)} %reshape.50.gain_ref) | copy-start | bytes 12292
  6.4 5.7 %copy-start.6 = (bf16[2048,64]{0,1:T(8,128)(2,1)S(1)}, bf16[2048,64]{0,1:T(8,128)(2,1)}, u32[]{:S(2)}) copy-start(bf16[2048,64]{0,1:T(8,128)(2,1)} %param.22) | copy-start | bytes 786436
  9.0 3.7 %copy-start.7 = (bf16[1,2048,64]{1,2,0:T(8,128)(2,1)S(1)}, bf16[1,2048,64]{1,2,0:T(8,128)(2,1)}, u32[]{:S(2)}) copy-start(bf16[1,2048,64]{1,2,0:T(8,128)(2,1)} %param.25) | copy-start | bytes 786436
  9.0 4.7 %copy-start.8 = (bf16[1,2048,64]{1,2,0:T(8,128)(2,1)S(1)}, bf16[1,2048,64]{1,2,0:T(8,128)(2,1)}, u32[]{:S(2)}) copy-start(bf16[1,2048,64]{1,2,0:T(8,128)(2,1)} %param.28) | copy-start | bytes 786436
  18.5 10.0 %copy-start = (f32[2048,128]{1,0:T(8,128)}, f32[2048,128]{1,0:T(8,128)S(1)}, u32[]{:S(2)}) copy-start(f32[2048,128]{1,0:T(8,128)S(1)} %get-tuple-element.9.down_ref.down_hbm) | copy-start | bytes 3145732
  18.5 10.0 %copy-start.1 = (f32[2048,128]{1,0:T(8,128)}, f32[2048,128]{1,0:T(8,128)S(1)}, u32[]{:S(2)}) copy-start(f32[2048,128]{1,0:T(8,128)S(1)} %get-tuple-element.10.up_ref.up_hbm) | copy-start | bytes 3145732
  18.5 10.0 %copy-start.2 = (f32[2048,128]{1,0:T(8,128)}, f32[2048,128]{1,0:T(8,128)S(1)}, u32[]{:S(2)}) copy-start(f32[2048,128]{1,0:T(8,128)S(1)} %get-tuple-element.11.cos_ref.cos_hbm) | copy-start | bytes 3145732
  28.6 0.8 copy-start.3
where the time goes:
time: 148 us; the launch traced here: 147 us
  Pallas kernels  123 us (83%)
  other arithmetic  9.88 us (7%)
  local copies, waits for them, and re-layouts  9.31 us (6%)
  matrix products  4.58 us (3%)
    pallas_call x1, Pallas kernels, per_device(): pl.pallas_call(functools.partial(exchange_kernel, planes), in_specs=[pl.B...  113 us
    pallas_call x1, Pallas kernels, per_device(): pl.pallas_call(sel_kernel, grid=(steps,), in_specs=[row_spec(width), full...  9.97 us
    unnamed x24, local copies, waits for them, and re-layouts  5.88 us
    dot_general x1, matrix products, per_device(): jnp.dot(gathered, out_weight, preferred_element_type=f32).astype(bf16)  4.58 us
    select_n x1, other arithmetic, per_device(): down = jnp.where(first, 0.0, sine)  3.78 us

commit v1 on v0

v1 whole, which is shorter than its diff:
```python
import functools

import jax
import jax.numpy as jnp
import numpy as np
from jax import lax
from jax.experimental import pallas as pl
from jax.experimental.pallas import tpu as pltpu
from jax.sharding import PartitionSpec as P

HEAD_DIM = 64
CMP_BLOCK = 32
SEL_BLOCK = 64
Q_BLOCK = 128
FAR_PICKS = 8
LANES = 2 * HEAD_DIM
PLANES = 4
ACROSS = 4
OWNERS = PLANES * ACROSS
RANKS = 8
MESH = pl.DeviceIdType.MESH

ROPE_BASE = 10000.0
norm_eps = 1e-06
MASKED = -1e30

MOVES = [(dz, dx) for dx in (2, 1, 3, 0) for dz in (2, 1, 3, 0) if (dz, dx) != (0, 0)]
EARLY = 5


def nt_dot(a, b):
    return lax.dot_general(a, b, (((1,), (1,)), ((), ())), preferred_element_type=jnp.float32)


def low_lanes(shape):
    return lax.broadcasted_iota(jnp.int32, shape, 1) < HEAD_DIM


def gate_lanes(gate, first, shape):
    return jnp.where(low_lanes(shape), gate[:, first : first + 1], gate[:, first + 1 : first + 2])


def merge(out, rows):
    low = low_lanes((rows, LANES))
    return jnp.where(low, pltpu.roll(out[:rows], HEAD_DIM, 1), out[rows:])


def layer_kernel(
    chosen_ref,
    gain_ref,
    ke_ref,
    ko_ref,
    ve_ref,
    vo_ref,
    lo_ref,
    hi_hbm,
    tok_hbm,
    wq_hbm,
    wsk_hbm,
    wsv_hbm,
    wck_hbm,
    wcv_hbm,
    wg_hbm,
    ki_hbm,
    vi_hbm,
    wo_hbm,
    out_ref,
    hi,
    tok,
    wq,
    raw,
    wt,
    ki,
    vi,
    wo,
    held,
    stage,
    got,
    qp,
    qt,
    ckv,
    gate,
    scales,
    sums,
    oc,
    mix,
    heard,
    pick_vm,
    pick_sm,
    near_sm,
    tok_sem,
    local_sem,
    send_sem,
    recv_sem,
    sum_send,
    sum_recv,
    mix_send,
    mix_recv,
):
    me, rank = lax.axis_index("kv"), lax.axis_index("tp")
    z, x = me // ACROSS, me % ACROSS
    rows, width = tok.shape
    tile = 512
    tiles = rows // tile
    q_blocks = rows // Q_BLOCK
    span = rows // SEL_BLOCK
    blocks = rows // CMP_BLOCK
    scale = HEAD_DIM ** (-0.5)

    sums[...] = jnp.zeros_like(sums)
    barrier = pltpu.get_barrier_semaphore()
    for d in range(1, OWNERS):
        pl.semaphore_signal(barrier, inc=1, device_id={"kv": (me + d) % OWNERS}, device_id_type=MESH)
    for d in range(1, RANKS):
        pl.semaphore_signal(barrier, inc=1, device_id={"tp": (rank + d) % RANKS}, device_id_type=MESH)

    loads = [
        (wq_hbm, wq),
        (wsk_hbm, raw.at[pl.ds(0, 64)]),
        (wsv_hbm, raw.at[pl.ds(64, 64)]),
        (wck_hbm, raw.at[pl.ds(128, 64)]),
        (wcv_hbm, raw.at[pl.ds(192, 64)]),
        (wg_hbm, raw.at[pl.ds(256, 32)]),
        (hi_hbm.at[pl.ds(pl.multiple_of(me * span, span), span)], hi),
        (ki_hbm, ki),
        (vi_hbm, vi),
        (wo_hbm, wo),
    ]
    copies = [pltpu.make_async_copy(a, b, local_sem.at[n]) for n, (a, b) in enumerate(loads)]
    tok_copies = [
        pltpu.make_async_copy(tok_hbm.at[pl.ds(n * tile, tile)], tok.at[pl.ds(n * tile, tile)], tok_sem.at[n])
        for n in range(tiles)
    ]
    for copy in copies[:7]:
        copy.start()
    for copy in tok_copies:
        copy.start()
    for copy in copies[7:]:
        copy.start()

    chosen = chosen_ref[...]
    mine = jnp.where(chosen // span == me, chosen % span, 0)
    pick_vm[0] = jnp.broadcast_to(jnp.sum(mine, axis=0, keepdims=True), chosen.shape)
    pick_vm[1] = chosen
    to_smem = pltpu.make_async_copy(pick_vm.at[0], pick_sm, local_sem.at[len(loads)])
    near_smem = pltpu.make_async_copy(pick_vm.at[1], near_sm, local_sem.at[len(loads) + 1])
    to_smem.start()
    near_smem.start()

    for copy in copies[:7]:
        copy.wait()

    gain = gain_ref[...].astype(jnp.float32)
    eye = (
        lax.broadcasted_iota(jnp.int32, (LANES, LANES), 0)
        == lax.broadcasted_iota(jnp.int32, (LANES, LANES), 1)
    ).astype(jnp.bfloat16)

    def weigh(source, first, count, target):
        def one(i, carry):
            r = pl.ds(pl.multiple_of(first + i * 16, 16), 16)
            t = pl.ds(pl.multiple_of(target + i * 16, 16), 16)
            wt[t] = (source[r].astype(jnp.float32) * gain).astype(jnp.bfloat16)
            return carry

        lax.fori_loop(0, count // 16, one, 0)

    weigh(raw, 0, 128, 0)
    for c in range(width // 256):
        cut = slice(c * 256, (c + 1) * 256)
        turned = nt_dot(eye, wq[cut])
        wt[128:256, cut] = (turned * gain[:, cut]).astype(jnp.bfloat16)

    first_half = lax.broadcasted_iota(jnp.int32, (1, LANES), 1) % HEAD_DIM < HEAD_DIM // 2
    quarter = HEAD_DIM // 2

    def turn(v, cosine, sine):
        swapped = jnp.where(first_half, pltpu.roll(v, LANES - quarter, 1), pltpu.roll(v, quarter, 1))
        return v * cosine + swapped * sine

    def project(i):
        at = pl.ds(i * tile, tile)
        v = tok[at]
        y = nt_dot(v, wt[0:256])
        w = v.astype(jnp.float32)
        inv = lax.rsqrt(jnp.mean(w * w, axis=-1, keepdims=True) + norm_eps)
        scales[at] = jnp.broadcast_to(inv, (tile, LANES))
        y = y * inv
        cos_lo, sin_lo = lo_ref[0:64], lo_ref[64:128]
        for g in range(tile // SEL_BLOCK):
            b = i * (tile // SEL_BLOCK) + g
            cut = slice(g * SEL_BLOCK, (g + 1) * SEL_BLOCK)
            cos_hi, sin_hi = hi[pl.ds(b, 1), 0:LANES], hi[pl.ds(b, 1), LANES : 2 * LANES]
            cosine = cos_hi * cos_lo - sin_hi * sin_lo
            sine = sin_hi * cos_lo + cos_hi * sin_lo
            sine = jnp.where(first_half, -sine, sine)
            part = y[cut, 0:LANES]
            low = low_lanes(part.shape)
            held[b] = jnp.where(low, turn(part, cosine, sine), part).astype(jnp.bfloat16)
            part = y[cut, LANES : 2 * LANES] * scale
            to = pl.ds(b * SEL_BLOCK, SEL_BLOCK)
            for ref, q in ((qp, part), (qt, turn(part, cosine, sine))):
                ref[0, to] = jnp.where(low, q, 0.0).astype(jnp.bfloat16)
                ref[1, to] = jnp.where(low, pltpu.roll(q, HEAD_DIM, 1), 0.0).astype(jnp.bfloat16)

    for i in range(tiles):
        tok_copies[i].wait()
        project(i)

    to_smem.wait()
    near_smem.wait()
    pl.semaphore_wait(barrier, OWNERS + RANKS - 2)

    def route(dz, dx):
        there = ((z + dz) % PLANES) * ACROSS + (x + dx) % ACROSS
        here = ((z - dz) % PLANES) * ACROSS + (x - dx) % ACROSS
        if dz == 0:
            return there, x + dx < ACROSS, here, x >= dx
        return there, z + dz < PLANES, here, z >= dz

    def block_copy(n, owner):
        there, sends, here, gets = route(*MOVES[n])
        copy = pltpu.make_async_remote_copy(
            src_ref=stage.at[n],
            dst_ref=got.at[owner],
            send_sem=send_sem.at[n],
            recv_sem=recv_sem.at[n],
            device_id={"kv": there},
            device_id_type=MESH,
        )
        return copy, there, sends, gets

    def gather(target, first):
        def one(j, carry):
            target[j] = held[pick_sm[0, first + j]]
            return carry

        lax.fori_loop(0, q_blocks, one, 0)

    def send_blocks(n):
        copy, there, sends, _ = block_copy(n, me)

        def go():
            gather(stage.at[n], there * q_blocks)
            copy.start()

        pl.when(sends)(go)

    for n in range(EARLY):
        send_blocks(n)

    weigh(raw, 128, 160, 256)

    def project_more(i, carry):
        at = pl.ds(pl.multiple_of(i * tile, tile), tile)
        y = nt_dot(tok[at], wt[256:416])
        inv = scales[at]
        ckv[at] = (y[:, 0:LANES] * inv).astype(jnp.bfloat16).astype(jnp.float32)
        gate[at] = jax.nn.sigmoid(y[:, LANES : LANES + 32] * inv[:, 0:32])
        return carry

    lax.fori_loop(0, tiles, project_more, 0)
    for copy in copies[7:9]:
        copy.wait()

    low = low_lanes((blocks, LANES))

    def summarize(is_value, e_ref, i_ref, o_ref):
        parts = []
        for c in range(0, CMP_BLOCK, 2):
            a = ckv[pl.ds(c, blocks, stride=CMP_BLOCK), :]
            b = ckv[pl.ds(c + 1, blocks, stride=CMP_BLOCK), :]
            if is_value:
                pair = jnp.where(low, pltpu.roll(a, HEAD_DIM, 1), b)
            else:
                pair = jnp.where(low, a, pltpu.roll(b, HEAD_DIM, 1))
            e = e_ref[c // 2 : c // 2 + 1, :].astype(jnp.float32)
            parts.append((pair + e).astype(jnp.bfloat16))
        flat = jnp.concatenate(parts, axis=1)
        hidden = jax.nn.gelu(nt_dot(flat, i_ref[...])).astype(jnp.bfloat16)
        return jnp.dot(hidden, o_ref[...], preferred_element_type=jnp.float32)

    sk = summarize(False, ke_ref, ki, ko_ref)
    sv = summarize(True, ve_ref, vi, vo_ref)
    sums[me] = jnp.concatenate([sk, sv], axis=1).astype(jnp.bfloat16)

    def sum_copy(n, owner):
        there, sends, here, gets = route(*MOVES[n])
        copy = pltpu.make_async_remote_copy(
            src_ref=sums.at[owner],
            dst_ref=sums.at[owner],
            send_sem=sum_send.at[n],
            recv_sem=sum_recv.at[n],
            device_id={"kv": there},
            device_id_type=MESH,
        )
        return copy, here, sends, gets

    for n in range(len(MOVES)):
        copy, _, sends, _ = sum_copy(n, me)
        pl.when(sends)(copy.start)
    for n in range(EARLY, len(MOVES)):
        send_blocks(n)
    gather(got.at[me], me * q_blocks)
    for n in range(len(MOVES)):
        _, here, _, gets = sum_copy(n, me)
        copy, _, _, _ = sum_copy(n, here)
        pl.when(gets)(copy.wait_recv)

    part = 256

    def compress(i, carry):
        at = pl.ds(pl.multiple_of(i * part, part), part)
        row = lax.broadcasted_iota(jnp.int32, (2 * part, 1), 0)
        pos = me * rows + i * part + jnp.where(row >= part, row - part, row)
        lane = lax.broadcasted_iota(jnp.int32, (1, OWNERS * blocks), 1)
        allowed = (lane + 1) * CMP_BLOCK - 1 <= pos
        keys = jnp.concatenate([sums[s] for s in range(OWNERS)], axis=0)
        q = jnp.concatenate([qp[0, at], qp[1, at]], axis=0)
        s = jnp.where(allowed, nt_dot(q, keys), MASKED)
        top = jnp.max(s, axis=-1, keepdims=True)
        e = jnp.exp(s - top)
        total = jnp.sum(e, axis=-1, keepdims=True)
        o = jnp.dot(e.astype(jnp.bfloat16), keys, preferred_element_type=jnp.float32)
        o = o * jnp.where(pos >= CMP_BLOCK - 1, 1.0 / total, 0.0)
        o = merge(o, part)
        g = pltpu.roll(pltpu_pad(gate[at]), LANES - 2 * rank, 1)
        oc[at] = o * gate_lanes(g, 0, o.shape)
        return carry

    def pltpu_pad(g):
        return jnp.concatenate([g, g, g, g], axis=1)

    lax.fori_loop(0, rows // part, compress, 0)

    rank_rows = rows // RANKS
    group = rank_rows // Q_BLOCK

    def mix_copy(step):
        target = (rank + 1 + step) % RANKS
        at = pl.ds(pl.multiple_of(target * rank_rows, rank_rows), rank_rows)
        return pltpu.make_async_remote_copy(
            src_ref=mix.at[at],
            dst_ref=heard.at[rank],
            send_sem=mix_send.at[step],
            recv_sem=mix_recv.at[step],
            device_id={"tp": target},
            device_id_type=MESH,
        )

    for n in range(len(MOVES)):
        _, _, here, _ = route(*MOVES[n])
        copy, _, _, gets = block_copy(n, here)
        pl.when(gets)(copy.wait_recv)

    def choose(step, carry):
        target = (rank + 1 + step) % RANKS
        for u in range(group):
            j = target * group + u
            at = pl.ds(pl.multiple_of(j * Q_BLOCK, Q_BLOCK), Q_BLOCK)
            own = j * (Q_BLOCK // SEL_BLOCK)
            parts = [held[own + b] for b in range(Q_BLOCK // SEL_BLOCK)]
            first = me * span + own
            biases = []
            for a in range(FAR_PICKS):
                pick = near_sm[a, me * q_blocks + j]
                usable = pick < first
                owner = jnp.where(usable, pick // span, me)
                parts.append(got[owner, j])
                biases.append(jnp.where(usable, 0.0, MASKED))
            keys = jnp.concatenate(parts, axis=0)
            q = jnp.concatenate([qt[0, at], qt[1, at]], axis=0)
            s = nt_dot(q, keys)
            row = lax.broadcasted_iota(jnp.int32, (2 * Q_BLOCK, Q_BLOCK), 0)
            row = jnp.where(row >= Q_BLOCK, row - Q_BLOCK, row)
            lane = lax.broadcasted_iota(jnp.int32, row.shape, 1)
            pieces = [jnp.where(lane > row, MASKED, s[:, :Q_BLOCK])]
            low = lax.broadcasted_iota(jnp.int32, (1, LANES), 1) < SEL_BLOCK
            for a in range(0, FAR_PICKS, 2):
                c = Q_BLOCK + a * SEL_BLOCK
                pieces.append(s[:, c : c + LANES] + jnp.where(low, biases[a], biases[a + 1]))
            s = jnp.concatenate(pieces, axis=1)
            top = jnp.max(s, axis=-1, keepdims=True)
            e = jnp.exp(s - top)
            total = jnp.sum(e, axis=-1, keepdims=True)
            o = jnp.dot(e.astype(jnp.bfloat16), keys, preferred_element_type=jnp.float32)
            o = merge(o * (1.0 / total), Q_BLOCK)
            g = pltpu.roll(pltpu_pad(gate[at]), LANES - 2 * rank, 1)
            mix[at] = (oc[at] + o * gate_lanes(g, 16, o.shape)).astype(jnp.bfloat16)
        pl.when(step > 0)(lambda: mix_copy(step - 1).start())
        return carry

    lax.fori_loop(0, RANKS, choose, 0)

    own_at = pl.ds(pl.multiple_of(rank * rank_rows, rank_rows), rank_rows)
    heard[rank] = mix[own_at]
    for n in range(len(MOVES)):
        copy, _, sends, _ = block_copy(n, me)
        pl.when(sends)(copy.wait_send)
        copy, _, sends, _ = sum_copy(n, me)
        pl.when(sends)(copy.wait_send)
    copies[9].wait()
    for step in range(RANKS - 1):
        mix_copy(step).wait_send()
        mix_copy(step).wait_recv()

    lhs = jnp.concatenate([heard[t] for t in range(RANKS)], axis=1)

    def finish(c, carry):
        at = pl.ds(pl.multiple_of(c * 512, 512), 512)
        out_ref[:, at] = jnp.dot(lhs, wo[:, at], preferred_element_type=jnp.float32).astype(jnp.bfloat16)
        return carry

    lax.fori_loop(0, width // 512, finish, 0)


def rope_tables(length):
    half = HEAD_DIM // 2
    inverse = ROPE_BASE ** (-(np.arange(half, dtype=np.float32)) / np.float32(half))
    inverse = np.tile(inverse.astype(np.float32).astype(np.float64), LANES // half)

    def table(positions):
        angle = positions.astype(np.float64)[:, None] * inverse[None, :]
        return np.cos(angle), np.sin(angle)

    low = np.concatenate(table(np.arange(SEL_BLOCK)), axis=0).astype(np.float32)
    high = np.concatenate(table(np.arange(length // SEL_BLOCK) * SEL_BLOCK), axis=1).astype(np.float32)
    return jnp.asarray(low), jnp.asarray(high)


def per_device(
    tokens,
    norm_gain,
    query_weight,
    cmp_key_weight,
    cmp_value_weight,
    sel_key_weight,
    sel_value_weight,
    branch_weight,
    key_embed,
    key_inner,
    key_outer,
    value_embed,
    value_inner,
    value_outer,
    out_weight,
    chosen,
):
    rows, width = tokens.shape
    f32, bf16 = jnp.float32, jnp.bfloat16
    low, high = rope_tables(rows * OWNERS)
    span = rows // SEL_BLOCK
    q_blocks = rows // Q_BLOCK
    blocks = rows // CMP_BLOCK
    rank_rows = rows // RANKS
    picks = chosen.shape[1]
    operands = (
        chosen[0].T,
        norm_gain.reshape(1, width),
        key_embed.reshape(CMP_BLOCK // 2, LANES),
        key_outer[0],
        value_embed.reshape(CMP_BLOCK // 2, LANES),
        value_outer[0],
        low,
        high,
        tokens,
        query_weight,
        sel_key_weight.T,
        sel_value_weight.T,
        cmp_key_weight.T,
        cmp_value_weight.T,
        branch_weight.transpose(0, 2, 1).reshape(32, width),
        key_inner[0].T,
        value_inner[0].T,
        out_weight,
    )
    vmem = pl.BlockSpec(memory_space=pltpu.VMEM)
    hbm = pl.BlockSpec(memory_space=pl.ANY)
    dma = pltpu.SemaphoreType.DMA
    moves = len(MOVES)
    return pl.pallas_call(
        layer_kernel,
        in_specs=[vmem] * 7 + [hbm] * 11,
        out_specs=vmem,
        out_shape=jax.ShapeDtypeStruct((rank_rows, width), bf16),
        scratch_shapes=[
            pltpu.VMEM((span, 2 * LANES), f32),
            pltpu.VMEM((rows, width), bf16),
            pltpu.VMEM((width, LANES), bf16),
            pltpu.VMEM((288, width), bf16),
            pltpu.VMEM((416, width), bf16),
            pltpu.VMEM((HEAD_DIM, width), bf16),
            pltpu.VMEM((HEAD_DIM, width), bf16),
            pltpu.VMEM(out_weight.shape, bf16),
            pltpu.VMEM((span, SEL_BLOCK, LANES), bf16),
            pltpu.VMEM((moves, q_blocks, SEL_BLOCK, LANES), bf16),
            pltpu.VMEM((OWNERS, q_blocks, SEL_BLOCK, LANES), bf16),
            pltpu.VMEM((2, rows, LANES), bf16),
            pltpu.VMEM((2, rows, LANES), bf16),
            pltpu.VMEM((rows, LANES), f32),
            pltpu.VMEM((rows, 32), f32),
            pltpu.VMEM((rows, LANES), f32),
            pltpu.VMEM((OWNERS, blocks, LANES), bf16),
            pltpu.VMEM((rows, LANES), f32),
            pltpu.VMEM((rows, LANES), bf16),
            pltpu.VMEM((RANKS, rank_rows, LANES), bf16),
            pltpu.VMEM((2, FAR_PICKS, picks), jnp.int32),
            pltpu.SMEM((FAR_PICKS, picks), jnp.int32),
            pltpu.SMEM((FAR_PICKS, picks), jnp.int32),
            dma((rows // 512,)),
            dma((12,)),
            dma((moves,)),
            dma((moves,)),
            dma((moves,)),
            dma((moves,)),
            dma((RANKS,)),
            dma((RANKS,)),
        ],
        compiler_params=pltpu.CompilerParams(
            collective_id=0, has_side_effects=True, vmem_limit_bytes=60 * 1024 * 1024
        ),
        cost_estimate=pl.CostEstimate(flops=int(4e10), bytes_accessed=int(2e7), transcendentals=0),
        name="layer",
    )(*operands)


def solution(mesh):
    placed = (
        P("kv", None),
        P(),
        P(None, "tp"),
        P(None, "tp"),
        P(None, "tp"),
        P(None, "tp"),
        P(None, "tp"),
        P(),
        P("tp", None, None),
        P("tp", None, None),
        P("tp", None, None),
        P("tp", None, None),
        P("tp", None, None),
        P("tp", None, None),
        P(),
        P("tp", None, None),
    )
    return jax.shard_map(
        per_device, mesh=mesh, in_specs=placed, out_specs=P(("kv", "tp"), None), check_vma=False
    )
```

time: 148 us -> 94.7 us (0.64)
  the two profiles are of different devices: /device:TPU:111 before, /device:TPU:13 now
where the time goes in v1:
time: 94.7 us; the launch traced here: 94.4 us
  Pallas kernels  88.1 us (93%)
  local copies, waits for them, and re-layouts  6.33 us (7%)
    pallas_call x1, Pallas kernels, per_device(): pl.pallas_call(layer_kernel, in_specs=[vmem] * 7 + [hbm] * 11, out_specs=...  88.1 us
    unnamed x1, local copies, waits for them, and re-layouts  2.3 us

profile of v1, /device:TPU:13, one launch (start us, length us, event | category | flops | bytes accessed | tf_op | source)
XLA Modules:
  0.0 94.4 jit_solution(14707466961022680513)
XLA Ops:
  0.0 1.4 %reshape.13.ke_ref = bf16[16,128]{1,0:T(8,128)(2,1)} reshape(bf16[1,32,64]{2,1,0:T(8,128)(2,1)} %param.26) | data formatting | bytes 8192 | tf_op jit(solution)/shard_map/reshape | solution.py:460
  1.4 1.4 %reshape.14.ve_ref = bf16[16,128]{1,0:T(8,128)(2,1)} reshape(bf16[1,32,64]{2,1,0:T(8,128)(2,1)} %param.29) | data formatting | bytes 8192 | tf_op jit(solution)/shard_map/reshape | solution.py:462
  2.7 1.3 %reshape.12.gain_ref = bf16[1,2048]{1,0:T(2,128)(2,1)} reshape(bf16[2048]{0:T(1024)(128)(2,1)} %param.19) | data formatting | bytes 8192 | tf_op jit(solution)/shard_map/reshape | solution.py:459
  4.0 88.1 %layer.1 = bf16[256,2048]{1,0:T(8,128)(2,1)} custom-call(s32[8,256]{1,0:T(8,128)} %bitcast.27, bf16[1,2048]{1,0:T(2,128)(2,1)} %reshape.12.gain_ref, bf16[16,128]{1,0:T(8,128)(2,1)} %reshape.13.ke_ref, bf16[64,64]{1,0:T(8,128)(2,1)} %bitcast.25, bf16[16,128]{1,0:T(8,128)(2,1)} %reshape.14.ve_ref, bf16[64,64]{1,0:T(8,128)(2,1)} %bitcast.26, ...), custom_call_target="tpu_custom_call" | custom-call | flops 40000000000 | bytes 20000000 | tf_op jit(solution)/shard_map/layer/pallas_call | solution.py:481
  92.1 2.3 %copy.20 = bf16[256,2048]{1,0:T(8,128)(2,1)} copy(bf16[256,2048]{1,0:T(8,128)(2,1)} %layer.1) | data formatting | bytes 2097152

commit v2 on v1

--- a/solution.py
+++ b/solution.py
@@ -25,7 +25,8 @@
 MASKED = -1e30
 
 MOVES = [(dz, dx) for dx in (2, 1, 3, 0) for dz in (2, 1, 3, 0) if (dz, dx) != (0, 0)]
-EARLY = 5
+OWN, NEAR, FAR, SKIP = range(4)
+HOPS = [(kind, dx) for kind in (OWN, NEAR, FAR) for dx in (2, 1, 3)] + [(SKIP, dx) for dx in (2, 1, 3, 0)]
 
 
 def nt_dot(a, b):
@@ -74,6 +75,8 @@
     vi,
     wo,
     held,
+    near,
+    far,
     stage,
     got,
     qp,
@@ -90,6 +93,8 @@
     near_sm,
     tok_sem,
     local_sem,
+    span_send,
+    span_recv,
     send_sem,
     recv_sem,
     sum_send,
@@ -139,8 +144,13 @@
         copy.start()
 
     chosen = chosen_ref[...]
-    mine = jnp.where(chosen // span == me, chosen % span, 0)
-    pick_vm[0] = jnp.broadcast_to(jnp.sum(mine, axis=0, keepdims=True), chosen.shape)
+    near_owner, far_owner = lax.rem(me + OWNERS - ACROSS, OWNERS), x
+    line = lax.broadcasted_iota(jnp.int32, chosen.shape, 0)
+    index = jnp.zeros(chosen.shape, jnp.int32)
+    for kind, owner in ((OWN, me), (NEAR, near_owner), (FAR, far_owner)):
+        inside = jnp.where(chosen // span == owner, chosen % span, 0)
+        index = jnp.where(line == kind, jnp.sum(inside, axis=0, keepdims=True), index)
+    pick_vm[0] = index
     pick_vm[1] = chosen
     to_smem = pltpu.make_async_copy(pick_vm.at[0], pick_sm, local_sem.at[len(loads)])
     near_smem = pltpu.make_async_copy(pick_vm.at[1], near_sm, local_sem.at[len(loads) + 1])
@@ -150,7 +160,7 @@
     for copy in copies[:7]:
         copy.wait()
 
-    gain = gain_ref[...].astype(jnp.float32)
+    gain = gain_ref[...].astype(jnp.float32).reshape(1, width)
     eye = (
         lax.broadcasted_iota(jnp.int32, (LANES, LANES), 0)
         == lax.broadcasted_iota(jnp.int32, (LANES, LANES), 1)
@@ -218,8 +228,32 @@
             return there, x + dx < ACROSS, here, x >= dx
         return there, z + dz < PLANES, here, z >= dz
 
-    def block_copy(n, owner):
-        there, sends, here, gets = route(*MOVES[n])
+    def span_copy(n):
+        step, sends, target = ((1, z < 3, near), (3, z == 0, far), (2, z == 0, far))[n]
+        there = lax.rem(me + step * ACROSS, OWNERS)
+        copy = pltpu.make_async_remote_copy(
+            src_ref=held,
+            dst_ref=target,
+            send_sem=span_send.at[n],
+            recv_sem=span_recv.at[min(n, 1)],
+            device_id={"kv": there},
+            device_id_type=MESH,
+        )
+        return copy, sends
+
+    def hop(n):
+        kind, dx = HOPS[n]
+        column = lax.rem(x + dx, ACROSS)
+        back = lax.rem(x + ACROSS - dx, ACROSS)
+        if kind == OWN:
+            owner, source, sends, gets = me, held, x + dx < ACROSS, x >= dx
+        elif kind == NEAR:
+            owner, source, sends, gets = near_owner, near, z >= 1, z >= 1
+        elif kind == FAR:
+            owner, source, sends, gets = far_owner, far, z >= 2, z >= 2
+        else:
+            owner, source, sends, gets = me, held, z == 1, z == 3
+        there = (3 if kind == SKIP else z) * ACROSS + column
         copy = pltpu.make_async_remote_copy(
             src_ref=stage.at[n],
             dst_ref=got.at[owner],
@@ -228,26 +262,31 @@
             device_id={"kv": there},
             device_id_type=MESH,
         )
-        return copy, there, sends, gets
-
-    def gather(target, first):
+        return copy, there, source, sends, gets
+
+    def gather(source, kind, target, first):
         def one(j, carry):
-            target[j] = held[pick_sm[0, first + j]]
+            target[j] = source[pick_sm[kind, first + j]]
             return carry
 
         lax.fori_loop(0, q_blocks, one, 0)
 
-    def send_blocks(n):
-        copy, there, sends, _ = block_copy(n, me)
-
-        def go():
-            gather(stage.at[n], there * q_blocks)
-            copy.start()
-
-        pl.when(sends)(go)
-
-    for n in range(EARLY):
-        send_blocks(n)
+    def send_hops(*kinds):
+        for n, (kind, dx) in enumerate(HOPS):
+            if kind in kinds:
+                copy, there, source, sends, _ = hop(n)
+
+                def go(n=n, kind=kind, copy=copy, there=there, source=source):
+                    gather(source, OWN if kind == SKIP else kind, stage.at[n], there * q_blocks)
+                    copy.start()
+
+                pl.when(sends)(go)
+
+    for n in range(3):
+        copy, sends = span_copy(n)
+        pl.when(sends)(copy.start)
+    send_hops(SKIP)
+    send_hops(OWN)
 
     weigh(raw, 128, 160, 256)
 
@@ -267,6 +306,7 @@
 
     def summarize(is_value, e_ref, i_ref, o_ref):
         parts = []
+        embed = e_ref[...].astype(jnp.float32)
         for c in range(0, CMP_BLOCK, 2):
             a = ckv[pl.ds(c, blocks, stride=CMP_BLOCK), :]
             b = ckv[pl.ds(c + 1, blocks, stride=CMP_BLOCK), :]
@@ -274,7 +314,7 @@
                 pair = jnp.where(low, pltpu.roll(a, HEAD_DIM, 1), b)
             else:
                 pair = jnp.where(low, a, pltpu.roll(b, HEAD_DIM, 1))
-            e = e_ref[c // 2 : c // 2 + 1, :].astype(jnp.float32)
+            e = jnp.concatenate([embed[c : c + 1], embed[c + 1 : c + 2]], axis=1)
             parts.append((pair + e).astype(jnp.bfloat16))
         flat = jnp.concatenate(parts, axis=1)
         hidden = jax.nn.gelu(nt_dot(flat, i_ref[...])).astype(jnp.bfloat16)
@@ -299,9 +339,20 @@
     for n in range(len(MOVES)):
         copy, _, sends, _ = sum_copy(n, me)
         pl.when(sends)(copy.start)
-    for n in range(EARLY, len(MOVES)):
-        send_blocks(n)
-    gather(got.at[me], me * q_blocks)
+    gather(held, OWN, got.at[me], me * q_blocks)
+
+    def pass_near():
+        span_copy(0)[0].wait_recv()
+        send_hops(NEAR)
+        gather(near, NEAR, got.at[near_owner], me * q_blocks)
+
+    def pass_far():
+        span_copy(1)[0].wait_recv()
+        send_hops(FAR)
+        gather(far, FAR, got.at[far_owner], me * q_blocks)
+
+    pl.when(z >= 1)(pass_near)
+    pl.when(z == 3)(pass_far)
     for n in range(len(MOVES)):
         _, here, _, gets = sum_copy(n, me)
         copy, _, _, _ = sum_copy(n, here)
@@ -331,7 +382,9 @@
     def pltpu_pad(g):
         return jnp.concatenate([g, g, g, g], axis=1)
 
-    lax.fori_loop(0, rows // part, compress, 0)
+    lax.fori_loop(0, 3, compress, 0)
+    pl.when(z == 2)(pass_far)
+    lax.fori_loop(3, rows // part, compress, 0)
 
     rank_rows = rows // RANKS
     group = rank_rows // Q_BLOCK
@@ -348,9 +401,8 @@
             device_id_type=MESH,
         )
 
-    for n in range(len(MOVES)):
-        _, _, here, _ = route(*MOVES[n])
-        copy, _, _, gets = block_copy(n, here)
+    for n in range(len(HOPS)):
+        copy, _, _, _, gets = hop(n)
         pl.when(gets)(copy.wait_recv)
 
     def choose(step, carry):
@@ -395,9 +447,13 @@
     own_at = pl.ds(pl.multiple_of(rank * rank_rows, rank_rows), rank_rows)
     heard[rank] = mix[own_at]
     for n in range(len(MOVES)):
-        copy, _, sends, _ = block_copy(n, me)
+        copy, _, sends, _ = sum_copy(n, me)
         pl.when(sends)(copy.wait_send)
-        copy, _, sends, _ = sum_copy(n, me)
+    for n in range(len(HOPS)):
+        copy, _, _, sends, _ = hop(n)
+        pl.when(sends)(copy.wait_send)
+    for n in range(3):
+        copy, sends = span_copy(n)
         pl.when(sends)(copy.wait_send)
     copies[9].wait()
     for step in range(RANKS - 1):
@@ -456,10 +512,10 @@
     picks = chosen.shape[1]
     operands = (
         chosen[0].T,
-        norm_gain.reshape(1, width),
-        key_embed.reshape(CMP_BLOCK // 2, LANES),
+        norm_gain,
+        key_embed[0],
         key_outer[0],
-        value_embed.reshape(CMP_BLOCK // 2, LANES),
+        value_embed[0],
         value_outer[0],
         low,
         high,
@@ -493,7 +549,9 @@
             pltpu.VMEM((HEAD_DIM, width), bf16),
             pltpu.VMEM(out_weight.shape, bf16),
             pltpu.VMEM((span, SEL_BLOCK, LANES), bf16),
-            pltpu.VMEM((moves, q_blocks, SEL_BLOCK, LANES), bf16),
+            pltpu.VMEM((span, SEL_BLOCK, LANES), bf16),
+            pltpu.VMEM((span, SEL_BLOCK, LANES), bf16),
+            pltpu.VMEM((len(HOPS), q_blocks, SEL_BLOCK, LANES), bf16),
             pltpu.VMEM((OWNERS, q_blocks, SEL_BLOCK, LANES), bf16),
             pltpu.VMEM((2, rows, LANES), bf16),
             pltpu.VMEM((2, rows, LANES), bf16),
@@ -509,8 +567,10 @@
             pltpu.SMEM((FAR_PICKS, picks), jnp.int32),
             dma((rows // 512,)),
             dma((12,)),
-            dma((moves,)),
-            dma((moves,)),
+            dma((3,)),
+            dma((2,)),
+            dma((len(HOPS),)),
+            dma((len(HOPS),)),
             dma((moves,)),
             dma((moves,)),
             dma((RANKS,)),

time: 94.7 us -> 80.1 us (0.85)
  the two profiles are of different devices: /device:TPU:13 before, /device:TPU:96 now
where the time goes in v2:
time: 80.1 us; the launch traced here: 78.6 us
  Pallas kernels  76.3 us (95%)
  local copies, waits for them, and re-layouts  2.3 us (3%)
    pallas_call x1, Pallas kernels, per_device(): pl.pallas_call(layer_kernel, in_specs=[vmem] * 7 + [hbm] * 11, out_specs=...  76.3 us
    unnamed x1, local copies, waits for them, and re-layouts  2.3 us

profile of v2, /device:TPU:96, one launch (start us, length us, event | category | flops | bytes accessed | tf_op | source)
XLA Modules:
  0.0 78.6 jit_solution(3791899775471743237)
XLA Ops:
  0.0 76.3 %layer.1 = bf16[256,2048]{1,0:T(8,128)(2,1)} custom-call(s32[8,256]{1,0:T(8,128)} %bitcast.29, bf16[2048]{0:T(1024)(128)(2,1)} %gain_ref.1, bf16[32,64]{1,0:T(8,128)(2,1)} %bitcast.30, bf16[64,64]{1,0:T(8,128)(2,1)} %bitcast.27, bf16[32,64]{1,0:T(8,128)(2,1)} %bitcast.31, bf16[64,64]{1,0:T(8,128)(2,1)} %bitcast.28, f32[128,128]{1,0:T(8,128)} %constant.4.clone.lo_ref, ...), custom_call_target="tpu_custom_call" | custom-call | flops 40000000000 | bytes 20000000 | tf_op jit(solution)/shard_map/layer/pallas_call | solution.py:537
  76.3 2.3 %copy.20 = bf16[256,2048]{1,0:T(8,128)(2,1)} copy(bf16[256,2048]{1,0:T(8,128)(2,1)} %layer.1) | data formatting | bytes 2097152

commit v3 on v2

--- a/solution.py
+++ b/solution.py
@@ -1,4 +1,4 @@
-import functools
+import math
 
 import jax
 import jax.numpy as jnp
@@ -26,7 +26,7 @@
 
 MOVES = [(dz, dx) for dx in (2, 1, 3, 0) for dz in (2, 1, 3, 0) if (dz, dx) != (0, 0)]
 OWN, NEAR, FAR, SKIP = range(4)
-HOPS = [(kind, dx) for kind in (OWN, NEAR, FAR) for dx in (2, 1, 3)] + [(SKIP, dx) for dx in (2, 1, 3, 0)]
+HOPS = [(kind, dx) for kind in (OWN, NEAR, FAR) for dx in (2, 1, 3)] + [(SKIP, dx) for dx in (0, 1, 3, 2)]
 
 
 def nt_dot(a, b):
@@ -85,6 +85,8 @@
     gate,
     scales,
     sums,
+    keys,
+    values,
     oc,
     mix,
     heard,
@@ -110,7 +112,7 @@
     q_blocks = rows // Q_BLOCK
     span = rows // SEL_BLOCK
     blocks = rows // CMP_BLOCK
-    scale = HEAD_DIM ** (-0.5)
+    scale = HEAD_DIM ** (-0.5) * math.log2(math.e)
 
     sums[...] = jnp.zeros_like(sums)
     barrier = pltpu.get_barrier_semaphore()
@@ -144,7 +146,7 @@
         copy.start()
 
     chosen = chosen_ref[...]
-    near_owner, far_owner = lax.rem(me + OWNERS - ACROSS, OWNERS), x
+    near_owner, far_owner = jnp.where(z == 0, me + ACROSS, me - ACROSS), x
     line = lax.broadcasted_iota(jnp.int32, chosen.shape, 0)
     index = jnp.zeros(chosen.shape, jnp.int32)
     for kind, owner in ((OWN, me), (NEAR, near_owner), (FAR, far_owner)):
@@ -182,6 +184,7 @@
         wt[128:256, cut] = (turned * gain[:, cut]).astype(jnp.bfloat16)
 
     first_half = lax.broadcasted_iota(jnp.int32, (1, LANES), 1) % HEAD_DIM < HEAD_DIM // 2
+    flag = (lax.broadcasted_iota(jnp.int32, (1, LANES), 1) == HEAD_DIM).astype(jnp.float32)
     quarter = HEAD_DIM // 2
 
     def turn(v, cosine, sine):
@@ -209,9 +212,9 @@
             held[b] = jnp.where(low, turn(part, cosine, sine), part).astype(jnp.bfloat16)
             part = y[cut, LANES : 2 * LANES] * scale
             to = pl.ds(b * SEL_BLOCK, SEL_BLOCK)
-            for ref, q in ((qp, part), (qt, turn(part, cosine, sine))):
-                ref[0, to] = jnp.where(low, q, 0.0).astype(jnp.bfloat16)
-                ref[1, to] = jnp.where(low, pltpu.roll(q, HEAD_DIM, 1), 0.0).astype(jnp.bfloat16)
+            for ref, q, rest in ((qp, part, flag), (qt, turn(part, cosine, sine), 0.0)):
+                ref[0, to] = jnp.where(low, q, rest).astype(jnp.bfloat16)
+                ref[1, to] = jnp.where(low, pltpu.roll(q, HEAD_DIM, 1), rest).astype(jnp.bfloat16)
 
     for i in range(tiles):
         tok_copies[i].wait()
@@ -229,17 +232,23 @@
         return there, z + dz < PLANES, here, z >= dz
 
     def span_copy(n):
-        step, sends, target = ((1, z < 3, near), (3, z == 0, far), (2, z == 0, far))[n]
-        there = lax.rem(me + step * ACROSS, OWNERS)
-        copy = pltpu.make_async_remote_copy(
-            src_ref=held,
-            dst_ref=target,
-            send_sem=span_send.at[n],
-            recv_sem=span_recv.at[min(n, 1)],
-            device_id={"kv": there},
-            device_id_type=MESH,
+        step, sends, source, target = (
+            (1, z < 3, held, near),
+            (3, z == 1, held, near),
+            (3, z == 0, held, far),
+            (3, z == 3, far, far),
+        )[n]
+        return (
+            pltpu.make_async_remote_copy(
+                src_ref=source,
+                dst_ref=target,
+                send_sem=span_send.at[n],
+                recv_sem=span_recv.at[n // 2],
+                device_id={"kv": lax.rem(me + step * ACROSS, OWNERS)},
+                device_id_type=MESH,
+            ),
+            sends,
         )
-        return copy, sends
 
     def hop(n):
         kind, dx = HOPS[n]
@@ -252,7 +261,7 @@
         elif kind == FAR:
             owner, source, sends, gets = far_owner, far, z >= 2, z >= 2
         else:
-            owner, source, sends, gets = me, held, z == 1, z == 3
+            owner, source, sends, gets = near_owner, near, z == 0, z == 3
         there = (3 if kind == SKIP else z) * ACROSS + column
         copy = pltpu.make_async_remote_copy(
             src_ref=stage.at[n],
@@ -277,7 +286,7 @@
                 copy, there, source, sends, _ = hop(n)
 
                 def go(n=n, kind=kind, copy=copy, there=there, source=source):
-                    gather(source, OWN if kind == SKIP else kind, stage.at[n], there * q_blocks)
+                    gather(source, NEAR if kind == SKIP else kind, stage.at[n], there * q_blocks)
                     copy.start()
 
                 pl.when(sends)(go)
@@ -285,7 +294,6 @@
     for n in range(3):
         copy, sends = span_copy(n)
         pl.when(sends)(copy.start)
-    send_hops(SKIP)
     send_hops(OWN)
 
     weigh(raw, 128, 160, 256)
@@ -342,15 +350,18 @@
     gather(held, OWN, got.at[me], me * q_blocks)
 
     def pass_near():
-        span_copy(0)[0].wait_recv()
         send_hops(NEAR)
         gather(near, NEAR, got.at[near_owner], me * q_blocks)
 
     def pass_far():
-        span_copy(1)[0].wait_recv()
+        span_copy(2)[0].wait_recv()
+        copy, sends = span_copy(3)
+        pl.when(sends)(copy.start)
         send_hops(FAR)
         gather(far, FAR, got.at[far_owner], me * q_blocks)
 
+    span_copy(0)[0].wait_recv()
+    send_hops(SKIP)
     pl.when(z >= 1)(pass_near)
     pl.when(z == 3)(pass_far)
     for n in range(len(MOVES)):
@@ -358,22 +369,29 @@
         copy, _, _, _ = sum_copy(n, here)
         pl.when(gets)(copy.wait_recv)
 
+    lane = lax.broadcasted_iota(jnp.int32, (blocks, LANES), 1)
+    for d in range(OWNERS):
+        owner = lax.rem(me + d, OWNERS)
+        both = sums[owner]
+        bar = jnp.where(owner > me, MASKED, 0.0).astype(jnp.bfloat16)
+        rows_at = slice(d * blocks, (d + 1) * blocks)
+        keys[rows_at] = jnp.where(lane == HEAD_DIM, bar, both)
+        values[rows_at] = jnp.where(lane < HEAD_DIM, jnp.ones_like(both), both)
+
     part = 256
 
     def compress(i, carry):
         at = pl.ds(pl.multiple_of(i * part, part), part)
         row = lax.broadcasted_iota(jnp.int32, (2 * part, 1), 0)
-        pos = me * rows + i * part + jnp.where(row >= part, row - part, row)
-        lane = lax.broadcasted_iota(jnp.int32, (1, OWNERS * blocks), 1)
-        allowed = (lane + 1) * CMP_BLOCK - 1 <= pos
-        keys = jnp.concatenate([sums[s] for s in range(OWNERS)], axis=0)
+        pos = i * part + jnp.where(row >= part, row - part, row)
+        lane = lax.broadcasted_iota(jnp.int32, (1, LANES), 1)
         q = jnp.concatenate([qp[0, at], qp[1, at]], axis=0)
-        s = jnp.where(allowed, nt_dot(q, keys), MASKED)
-        top = jnp.max(s, axis=-1, keepdims=True)
-        e = jnp.exp(s - top)
-        total = jnp.sum(e, axis=-1, keepdims=True)
-        o = jnp.dot(e.astype(jnp.bfloat16), keys, preferred_element_type=jnp.float32)
-        o = o * jnp.where(pos >= CMP_BLOCK - 1, 1.0 / total, 0.0)
+        s = nt_dot(q, keys[...])
+        own = jnp.where((lane >= blocks) | ((lane + 1) * CMP_BLOCK - 1 <= pos), s[:, :LANES], MASKED)
+        s = jnp.concatenate([own, s[:, LANES:]], axis=1)
+        e = jnp.exp2(s - jnp.max(s, axis=-1, keepdims=True))
+        o = jnp.dot(e.astype(jnp.bfloat16), values[...], preferred_element_type=jnp.float32)
+        o = jnp.where(me * rows + pos >= CMP_BLOCK - 1, o * pltpu.roll(1.0 / o, HEAD_DIM, 1), 0.0)
         o = merge(o, part)
         g = pltpu.roll(pltpu_pad(gate[at]), LANES - 2 * rank, 1)
         oc[at] = o * gate_lanes(g, 0, o.shape)
@@ -420,9 +438,9 @@
                 owner = jnp.where(usable, pick // span, me)
                 parts.append(got[owner, j])
                 biases.append(jnp.where(usable, 0.0, MASKED))
-            keys = jnp.concatenate(parts, axis=0)
+            both = jnp.concatenate(parts, axis=0)
             q = jnp.concatenate([qt[0, at], qt[1, at]], axis=0)
-            s = nt_dot(q, keys)
+            s = nt_dot(q, both)
             row = lax.broadcasted_iota(jnp.int32, (2 * Q_BLOCK, Q_BLOCK), 0)
             row = jnp.where(row >= Q_BLOCK, row - Q_BLOCK, row)
             lane = lax.broadcasted_iota(jnp.int32, row.shape, 1)
@@ -433,10 +451,10 @@
                 pieces.append(s[:, c : c + LANES] + jnp.where(low, biases[a], biases[a + 1]))
             s = jnp.concatenate(pieces, axis=1)
             top = jnp.max(s, axis=-1, keepdims=True)
-            e = jnp.exp(s - top)
-            total = jnp.sum(e, axis=-1, keepdims=True)
-            o = jnp.dot(e.astype(jnp.bfloat16), keys, preferred_element_type=jnp.float32)
-            o = merge(o * (1.0 / total), Q_BLOCK)
+            e = jnp.exp2(s - top)
+            both = jnp.where(low_lanes(both.shape), jnp.ones_like(both), both)
+            o = jnp.dot(e.astype(jnp.bfloat16), both, preferred_element_type=jnp.float32)
+            o = merge(o * pltpu.roll(1.0 / o, HEAD_DIM, 1), Q_BLOCK)
             g = pltpu.roll(pltpu_pad(gate[at]), LANES - 2 * rank, 1)
             mix[at] = (oc[at] + o * gate_lanes(g, 16, o.shape)).astype(jnp.bfloat16)
         pl.when(step > 0)(lambda: mix_copy(step - 1).start())
@@ -452,7 +470,7 @@
     for n in range(len(HOPS)):
         copy, _, _, sends, _ = hop(n)
         pl.when(sends)(copy.wait_send)
-    for n in range(3):
+    for n in range(4):
         copy, sends = span_copy(n)
         pl.when(sends)(copy.wait_send)
     copies[9].wait()
@@ -538,7 +556,7 @@
         layer_kernel,
         in_specs=[vmem] * 7 + [hbm] * 11,
         out_specs=vmem,
-        out_shape=jax.ShapeDtypeStruct((rank_rows, width), bf16),
+        out_shape=pltpu.VMEM((rank_rows, width), bf16),
         scratch_shapes=[
             pltpu.VMEM((span, 2 * LANES), f32),
             pltpu.VMEM((rows, width), bf16),
@@ -559,6 +577,8 @@
             pltpu.VMEM((rows, 32), f32),
             pltpu.VMEM((rows, LANES), f32),
             pltpu.VMEM((OWNERS, blocks, LANES), bf16),
+            pltpu.VMEM((OWNERS * blocks, LANES), bf16),
+            pltpu.VMEM((OWNERS * blocks, LANES), bf16),
             pltpu.VMEM((rows, LANES), f32),
             pltpu.VMEM((rows, LANES), bf16),
             pltpu.VMEM((RANKS, rank_rows, LANES), bf16),
@@ -567,7 +587,7 @@
             pltpu.SMEM((FAR_PICKS, picks), jnp.int32),
             dma((rows // 512,)),
             dma((12,)),
-            dma((3,)),
+            dma((4,)),
             dma((2,)),
             dma((len(HOPS),)),
             dma((len(HOPS),)),

time: 80.1 us -> 68.9 us (0.86)
  the two profiles are of different devices: /device:TPU:96 before, /device:TPU:73 now
where the time goes in v3:
time: 68.9 us; the launch traced here: 68.8 us
  Pallas kernels  67.8 us (98%)
  local copies, waits for them, and re-layouts  0.97 us (1%)
    pallas_call x1, Pallas kernels, per_device(): pl.pallas_call(layer_kernel, in_specs=[vmem] * 7 + [hbm] * 11, out_specs=...  67.8 us

profile of v3, /device:TPU:73, one launch (start us, length us, event | category | flops | bytes accessed | tf_op | source)
XLA Modules:
  0.0 68.8 jit_solution(6490070889263077155)
XLA Ops:
  0.0 67.8 %layer.1 = bf16[256,2048]{1,0:T(8,128)(2,1)S(1)} custom-call(s32[8,256]{1,0:T(8,128)} %bitcast.29, bf16[2048]{0:T(1024)(128)(2,1)} %gain_ref.1, bf16[32,64]{1,0:T(8,128)(2,1)} %bitcast.30, bf16[64,64]{1,0:T(8,128)(2,1)} %bitcast.27, bf16[32,64]{1,0:T(8,128)(2,1)} %bitcast.31, bf16[64,64]{1,0:T(8,128)(2,1)} %bitcast.28, f32[128,128]{1,0:T(8,128)} %constant.4.clone.lo_ref, ...), custom_call_target="tpu_custom_call" | custom-call | flops 40000000000 | bytes 20000000 | tf_op jit(solution)/shard_map/layer/pallas_call | solution.py:555
  67.8 1.0 %copy.20 = bf16[256,2048]{1,0:T(8,128)(2,1)} copy(bf16[256,2048]{1,0:T(8,128)(2,1)S(1)} %layer.1) | data formatting | bytes 2097152

commit v4 on v3

--- a/solution.py
+++ b/solution.py
@@ -1,3 +1,4 @@
+import functools
 import math
 
 import jax
@@ -353,13 +354,16 @@
         send_hops(NEAR)
         gather(near, NEAR, got.at[near_owner], me * q_blocks)
 
+    def hand_back():
+        span_copy(2)[0].wait_recv()
+        span_copy(3)[0].start()
+
     def pass_far():
-        span_copy(2)[0].wait_recv()
-        copy, sends = span_copy(3)
-        pl.when(sends)(copy.start)
+        pl.when(z == 2)(span_copy(2)[0].wait_recv)
         send_hops(FAR)
         gather(far, FAR, got.at[far_owner], me * q_blocks)
 
+    pl.when(z == 3)(hand_back)
     span_copy(0)[0].wait_recv()
     send_hops(SKIP)
     pl.when(z >= 1)(pass_near)
@@ -382,17 +386,19 @@
 
     def compress(i, carry):
         at = pl.ds(pl.multiple_of(i * part, part), part)
-        row = lax.broadcasted_iota(jnp.int32, (2 * part, 1), 0)
-        pos = i * part + jnp.where(row >= part, row - part, row)
+        pos = i * part + lax.broadcasted_iota(jnp.int32, (part, 1), 0)
         lane = lax.broadcasted_iota(jnp.int32, (1, LANES), 1)
-        q = jnp.concatenate([qp[0, at], qp[1, at]], axis=0)
-        s = nt_dot(q, keys[...])
-        own = jnp.where((lane >= blocks) | ((lane + 1) * CMP_BLOCK - 1 <= pos), s[:, :LANES], MASKED)
-        s = jnp.concatenate([own, s[:, LANES:]], axis=1)
-        e = jnp.exp2(s - jnp.max(s, axis=-1, keepdims=True))
-        o = jnp.dot(e.astype(jnp.bfloat16), values[...], preferred_element_type=jnp.float32)
-        o = jnp.where(me * rows + pos >= CMP_BLOCK - 1, o * pltpu.roll(1.0 / o, HEAD_DIM, 1), 0.0)
-        o = merge(o, part)
+        scored = [nt_dot(qp[h, at], keys[...]) for h in range(2)]
+        outs = []
+        for s in scored:
+            own = jnp.where((lane >= blocks) | ((lane + 1) * CMP_BLOCK - 1 <= pos), s[:, :LANES], MASKED)
+            pieces = [own] + [s[:, c : c + LANES] for c in range(LANES, OWNERS * blocks, LANES)]
+            top = jnp.max(functools.reduce(jnp.maximum, pieces), axis=-1, keepdims=True)
+            e = jnp.concatenate([jnp.exp2(p - top).astype(jnp.bfloat16) for p in pieces], axis=1)
+            o = jnp.dot(e, values[...], preferred_element_type=jnp.float32)
+            outs.append(o * pltpu.roll(1.0 / o, HEAD_DIM, 1))
+        o = jnp.where(low_lanes(outs[0].shape), pltpu.roll(outs[0], HEAD_DIM, 1), outs[1])
+        o = jnp.where(me * rows + pos >= CMP_BLOCK - 1, o, 0.0)
         g = pltpu.roll(pltpu_pad(gate[at]), LANES - 2 * rank, 1)
         oc[at] = o * gate_lanes(g, 0, o.shape)
         return carry
@@ -423,40 +429,51 @@
         copy, _, _, _, gets = hop(n)
         pl.when(gets)(copy.wait_recv)
 
+    own_row = lax.broadcasted_iota(jnp.int32, (2 * Q_BLOCK, Q_BLOCK), 0)
+    own_row = jnp.where(own_row >= Q_BLOCK, own_row - Q_BLOCK, own_row)
+    later = lax.broadcasted_iota(jnp.int32, own_row.shape, 1) > own_row
+    low_lane = lax.broadcasted_iota(jnp.int32, (1, LANES), 1) < SEL_BLOCK
+
+    def score(j):
+        at = pl.ds(pl.multiple_of(j * Q_BLOCK, Q_BLOCK), Q_BLOCK)
+        own = j * (Q_BLOCK // SEL_BLOCK)
+        parts = [held[own + b] for b in range(Q_BLOCK // SEL_BLOCK)]
+        first = me * span + own
+        biases = []
+        for a in range(FAR_PICKS):
+            pick = near_sm[a, me * q_blocks + j]
+            usable = pick < first
+            owner = jnp.where(usable, pick // span, me)
+            parts.append(got[owner, j])
+            biases.append(jnp.where(usable, 0.0, MASKED))
+        both = jnp.concatenate(parts, axis=0)
+        q = jnp.concatenate([qt[0, at], qt[1, at]], axis=0)
+        return nt_dot(q, both), both, biases
+
+    def weights(s, biases):
+        pieces = [jnp.where(later, MASKED, s[:, :Q_BLOCK])]
+        for a in range(0, FAR_PICKS, 2):
+            c = Q_BLOCK + a * SEL_BLOCK
+            pieces.append(s[:, c : c + LANES] + jnp.where(low_lane, biases[a], biases[a + 1]))
+        top = functools.reduce(jnp.maximum, pieces)
+        top = jnp.max(top, axis=-1, keepdims=True)
+        return [jnp.exp2(p - top).astype(jnp.bfloat16) for p in pieces]
+
+    def settle(j, e, both):
+        at = pl.ds(pl.multiple_of(j * Q_BLOCK, Q_BLOCK), Q_BLOCK)
+        both = jnp.where(low_lanes(both.shape), jnp.ones_like(both), both)
+        o = jnp.dot(jnp.concatenate(e, axis=1), both, preferred_element_type=jnp.float32)
+        o = merge(o * pltpu.roll(1.0 / o, HEAD_DIM, 1), Q_BLOCK)
+        g = pltpu.roll(pltpu_pad(gate[at]), LANES - 2 * rank, 1)
+        mix[at] = (oc[at] + o * gate_lanes(g, 16, o.shape)).astype(jnp.bfloat16)
+
     def choose(step, carry):
         target = (rank + 1 + step) % RANKS
-        for u in range(group):
-            j = target * group + u
-            at = pl.ds(pl.multiple_of(j * Q_BLOCK, Q_BLOCK), Q_BLOCK)
-            own = j * (Q_BLOCK // SEL_BLOCK)
-            parts = [held[own + b] for b in range(Q_BLOCK // SEL_BLOCK)]
-            first = me * span + own
-            biases = []
-            for a in range(FAR_PICKS):
-                pick = near_sm[a, me * q_blocks + j]
-                usable = pick < first
-                owner = jnp.where(usable, pick // span, me)
-                parts.append(got[owner, j])
-                biases.append(jnp.where(usable, 0.0, MASKED))
-            both = jnp.concatenate(parts, axis=0)
-            q = jnp.concatenate([qt[0, at], qt[1, at]], axis=0)
-            s = nt_dot(q, both)
-            row = lax.broadcasted_iota(jnp.int32, (2 * Q_BLOCK, Q_BLOCK), 0)
-            row = jnp.where(row >= Q_BLOCK, row - Q_BLOCK, row)
-            lane = lax.broadcasted_iota(jnp.int32, row.shape, 1)
-            pieces = [jnp.where(lane > row, MASKED, s[:, :Q_BLOCK])]
-            low = lax.broadcasted_iota(jnp.int32, (1, LANES), 1) < SEL_BLOCK
-            for a in range(0, FAR_PICKS, 2):
-                c = Q_BLOCK + a * SEL_BLOCK
-                pieces.append(s[:, c : c + LANES] + jnp.where(low, biases[a], biases[a + 1]))
-            s = jnp.concatenate(pieces, axis=1)
-            top = jnp.max(s, axis=-1, keepdims=True)
-            e = jnp.exp2(s - top)
-            both = jnp.where(low_lanes(both.shape), jnp.ones_like(both), both)
-            o = jnp.dot(e.astype(jnp.bfloat16), both, preferred_element_type=jnp.float32)
-            o = merge(o * pltpu.roll(1.0 / o, HEAD_DIM, 1), Q_BLOCK)
-            g = pltpu.roll(pltpu_pad(gate[at]), LANES - 2 * rank, 1)
-            mix[at] = (oc[at] + o * gate_lanes(g, 16, o.shape)).astype(jnp.bfloat16)
+        js = [target * group + u for u in range(group)]
+        scored = [score(j) for j in js]
+        es = [weights(s, biases) for s, _, biases in scored]
+        for j, e, (_, both, _) in zip(js, es, scored):
+            settle(j, e, both)
         pl.when(step > 0)(lambda: mix_copy(step - 1).start())
         return carry
 

time: 68.9 us -> 65.3 us (0.948)
  Pallas kernels: 67.8 us -> 64.1 us
    pallas_call x1, Pallas kernels: 67.8 us -> 64.1 us  [per_device(): pl.pallas_call(layer_kernel, in_specs=[vmem] * 7 + [hbm] * 11, out_specs=...]
where the time goes in v4:
time: 65.3 us; the launch traced here: 65.1 us
  Pallas kernels  64.1 us (98%)
  local copies, waits for them, and re-layouts  0.97 us (1%)
    pallas_call x1, Pallas kernels, per_device(): pl.pallas_call(layer_kernel, in_specs=[vmem] * 7 + [hbm] * 11, out_specs=...  64.1 us

profile of v4, /device:TPU:73, one launch (start us, length us, event | category | flops | bytes accessed | tf_op | source)
XLA Modules:
  0.0 65.1 jit_solution(14818676913240328836)
XLA Ops:
  0.0 64.1 %layer.1 = bf16[256,2048]{1,0:T(8,128)(2,1)S(1)} custom-call(s32[8,256]{1,0:T(8,128)} %bitcast.29, bf16[2048]{0:T(1024)(128)(2,1)} %gain_ref.1, bf16[32,64]{1,0:T(8,128)(2,1)} %bitcast.30, bf16[64,64]{1,0:T(8,128)(2,1)} %bitcast.27, bf16[32,64]{1,0:T(8,128)(2,1)} %bitcast.31, bf16[64,64]{1,0:T(8,128)(2,1)} %bitcast.28, f32[128,128]{1,0:T(8,128)} %constant.4.clone.lo_ref, ...), custom_call_target="tpu_custom_call" | custom-call | flops 40000000000 | bytes 20000000 | tf_op jit(solution)/shard_map/layer/pallas_call | solution.py:572
  64.1 1.0 %copy.20 = bf16[256,2048]{1,0:T(8,128)(2,1)} copy(bf16[256,2048]{1,0:T(8,128)(2,1)S(1)} %layer.1) | data formatting | bytes 2097152

commit v5 on v4

--- a/solution.py
+++ b/solution.py
@@ -27,6 +27,8 @@
 
 MOVES = [(dz, dx) for dx in (2, 1, 3, 0) for dz in (2, 1, 3, 0) if (dz, dx) != (0, 0)]
 OWN, NEAR, FAR, SKIP = range(4)
+LATE = [(FAR, 1), (FAR, 3), (SKIP, 3), (SKIP, 2)]
+EARLY_PICKS = FAR_PICKS - len(LATE)
 HOPS = [(kind, dx) for kind in (OWN, NEAR, FAR) for dx in (2, 1, 3)] + [(SKIP, dx) for dx in (0, 1, 3, 2)]
 
 
@@ -80,6 +82,9 @@
     far,
     stage,
     got,
+    late,
+    first_out,
+    first_top,
     qp,
     qt,
     ckv,
@@ -154,7 +159,26 @@
         inside = jnp.where(chosen // span == owner, chosen % span, 0)
         index = jnp.where(line == kind, jnp.sum(inside, axis=0, keepdims=True), index)
     pick_vm[0] = index
-    pick_vm[1] = chosen
+    at_block = lax.broadcasted_iota(jnp.int32, chosen.shape, 1) * (Q_BLOCK // SEL_BLOCK)
+    usable = chosen < at_block
+    owner = chosen // span
+    away = lax.rem(x + ACROSS - lax.rem(owner, ACROSS), ACROSS)
+    place = jnp.full(chosen.shape, -1, jnp.int32)
+    for n, (kind, dx) in enumerate(LATE):
+        home, receives = (0, z >= 2) if kind == FAR else (1, z == 3)
+        hit = (owner // ACROSS == home) & (away == dx) & usable
+        place = jnp.where(hit & receives, n, place)
+    code = jnp.where(usable, jnp.where(place >= 0, 32 + place, owner), 64 + me)
+    slow = (place >= 0).astype(jnp.int32)
+    quick_count = FAR_PICKS - jnp.sum(slow, axis=0, keepdims=True)
+    table = jnp.zeros(chosen.shape, jnp.int32)
+    before = jnp.zeros((1, chosen.shape[1]), jnp.int32)
+    for a in range(FAR_PICKS):
+        is_slow = slow[a : a + 1]
+        rank_of = jnp.where(is_slow > 0, quick_count + before, a - before)
+        table = jnp.where(line == rank_of, code[a : a + 1], table)
+        before = before + is_slow
+    pick_vm[1] = table
     to_smem = pltpu.make_async_copy(pick_vm.at[0], pick_sm, local_sem.at[len(loads)])
     near_smem = pltpu.make_async_copy(pick_vm.at[1], near_sm, local_sem.at[len(loads) + 1])
     to_smem.start()
@@ -217,14 +241,6 @@
                 ref[0, to] = jnp.where(low, q, rest).astype(jnp.bfloat16)
                 ref[1, to] = jnp.where(low, pltpu.roll(q, HEAD_DIM, 1), rest).astype(jnp.bfloat16)
 
-    for i in range(tiles):
-        tok_copies[i].wait()
-        project(i)
-
-    to_smem.wait()
-    near_smem.wait()
-    pl.semaphore_wait(barrier, OWNERS + RANKS - 2)
-
     def route(dz, dx):
         there = ((z + dz) % PLANES) * ACROSS + (x + dx) % ACROSS
         here = ((z - dz) % PLANES) * ACROSS + (x - dx) % ACROSS
@@ -232,24 +248,37 @@
             return there, x + dx < ACROSS, here, x >= dx
         return there, z + dz < PLANES, here, z >= dz
 
-    def span_copy(n):
+    def span_copy(n, c):
         step, sends, source, target = (
             (1, z < 3, held, near),
             (3, z == 1, held, near),
             (3, z == 0, held, far),
             (3, z == 3, far, far),
         )[n]
+        at = pl.ds(c * (span // tiles), span // tiles)
         return (
             pltpu.make_async_remote_copy(
-                src_ref=source,
-                dst_ref=target,
-                send_sem=span_send.at[n],
-                recv_sem=span_recv.at[n // 2],
+                src_ref=source.at[at],
+                dst_ref=target.at[at],
+                send_sem=span_send.at[n, c],
+                recv_sem=span_recv.at[n // 2, c],
                 device_id={"kv": lax.rem(me + step * ACROSS, OWNERS)},
                 device_id_type=MESH,
             ),
             sends,
         )
+
+    for i in range(tiles):
+        tok_copies[i].wait()
+        project(i)
+        if i == 0:
+            pl.semaphore_wait(barrier, OWNERS + RANKS - 2)
+        for n in range(3):
+            copy, sends = span_copy(n, i)
+            pl.when(sends)(copy.start)
+
+    to_smem.wait()
+    near_smem.wait()
 
     def hop(n):
         kind, dx = HOPS[n]
@@ -266,7 +295,7 @@
         there = (3 if kind == SKIP else z) * ACROSS + column
         copy = pltpu.make_async_remote_copy(
             src_ref=stage.at[n],
-            dst_ref=got.at[owner],
+            dst_ref=late.at[LATE.index(HOPS[n])] if HOPS[n] in LATE else got.at[owner],
             send_sem=send_sem.at[n],
             recv_sem=recv_sem.at[n],
             device_id={"kv": there},
@@ -292,22 +321,24 @@
 
                 pl.when(sends)(go)
 
-    for n in range(3):
-        copy, sends = span_copy(n)
-        pl.when(sends)(copy.start)
     send_hops(OWN)
 
     weigh(raw, 128, 160, 256)
 
-    def project_more(i, carry):
-        at = pl.ds(pl.multiple_of(i * tile, tile), tile)
+    def project_more(i):
+        at = pl.ds(i * tile, tile)
         y = nt_dot(tok[at], wt[256:416])
         inv = scales[at]
         ckv[at] = (y[:, 0:LANES] * inv).astype(jnp.bfloat16).astype(jnp.float32)
         gate[at] = jax.nn.sigmoid(y[:, LANES : LANES + 32] * inv[:, 0:32])
-        return carry
-
-    lax.fori_loop(0, tiles, project_more, 0)
+
+    def hand_back(c):
+        span_copy(2, c)[0].wait_recv()
+        span_copy(3, c)[0].start()
+
+    for c in range(tiles):
+        project_more(c)
+        pl.when(z == 3)(functools.partial(hand_back, c))
     for copy in copies[7:9]:
         copy.wait()
 
@@ -354,20 +385,17 @@
         send_hops(NEAR)
         gather(near, NEAR, got.at[near_owner], me * q_blocks)
 
-    def hand_back():
-        span_copy(2)[0].wait_recv()
-        span_copy(3)[0].start()
-
     def pass_far():
-        pl.when(z == 2)(span_copy(2)[0].wait_recv)
+        for c in range(tiles):
+            pl.when(z == 2)(span_copy(2, c)[0].wait_recv)
         send_hops(FAR)
         gather(far, FAR, got.at[far_owner], me * q_blocks)
 
-    pl.when(z == 3)(hand_back)
-    span_copy(0)[0].wait_recv()
+    for c in range(tiles):
+        span_copy(0, c)[0].wait_recv()
     send_hops(SKIP)
     pl.when(z >= 1)(pass_near)
-    pl.when(z == 3)(pass_far)
+    pl.when(z >= 2)(pass_far)
     for n in range(len(MOVES)):
         _, here, _, gets = sum_copy(n, me)
         copy, _, _, _ = sum_copy(n, here)
@@ -406,15 +434,17 @@
     def pltpu_pad(g):
         return jnp.concatenate([g, g, g, g], axis=1)
 
-    lax.fori_loop(0, 3, compress, 0)
-    pl.when(z == 2)(pass_far)
-    lax.fori_loop(3, rows // part, compress, 0)
+    lax.fori_loop(0, rows // part, compress, 0)
 
     rank_rows = rows // RANKS
     group = rank_rows // Q_BLOCK
 
+    def mix_target(step):
+        mask = RANKS - 1 - step
+        return sum((rank // w + mask // w) % 2 * w for w in (4, 2, 1))
+
     def mix_copy(step):
-        target = (rank + 1 + step) % RANKS
+        target = mix_target(step)
         at = pl.ds(pl.multiple_of(target * rank_rows, rank_rows), rank_rows)
         return pltpu.make_async_remote_copy(
             src_ref=mix.at[at],
@@ -425,56 +455,89 @@
             device_id_type=MESH,
         )
 
-    for n in range(len(HOPS)):
-        copy, _, _, _, gets = hop(n)
-        pl.when(gets)(copy.wait_recv)
-
     own_row = lax.broadcasted_iota(jnp.int32, (2 * Q_BLOCK, Q_BLOCK), 0)
     own_row = jnp.where(own_row >= Q_BLOCK, own_row - Q_BLOCK, own_row)
     later = lax.broadcasted_iota(jnp.int32, own_row.shape, 1) > own_row
     low_lane = lax.broadcasted_iota(jnp.int32, (1, LANES), 1) < SEL_BLOCK
 
-    def score(j):
+    def arrive(is_late):
+        for n, key in enumerate(HOPS):
+            if (key in LATE) == is_late:
+                copy, _, _, _, gets = hop(n)
+                pl.when(gets)(copy.wait_recv)
+
+    def queries(j):
         at = pl.ds(pl.multiple_of(j * Q_BLOCK, Q_BLOCK), Q_BLOCK)
+        return jnp.concatenate([qt[0, at], qt[1, at]], axis=0)
+
+    def with_ones(both):
+        return jnp.where(low_lanes(both.shape), jnp.ones_like(both), both)
+
+    def bias_of(a, j):
+        return jnp.where(near_sm[a, me * q_blocks + j] < 64, 0.0, MASKED)
+
+    def first_blocks(j):
         own = j * (Q_BLOCK // SEL_BLOCK)
         parts = [held[own + b] for b in range(Q_BLOCK // SEL_BLOCK)]
-        first = me * span + own
-        biases = []
-        for a in range(FAR_PICKS):
-            pick = near_sm[a, me * q_blocks + j]
-            usable = pick < first
-            owner = jnp.where(usable, pick // span, me)
-            parts.append(got[owner, j])
-            biases.append(jnp.where(usable, 0.0, MASKED))
-        both = jnp.concatenate(parts, axis=0)
-        q = jnp.concatenate([qt[0, at], qt[1, at]], axis=0)
-        return nt_dot(q, both), both, biases
-
-    def weights(s, biases):
-        pieces = [jnp.where(later, MASKED, s[:, :Q_BLOCK])]
-        for a in range(0, FAR_PICKS, 2):
-            c = Q_BLOCK + a * SEL_BLOCK
-            pieces.append(s[:, c : c + LANES] + jnp.where(low_lane, biases[a], biases[a + 1]))
-        top = functools.reduce(jnp.maximum, pieces)
-        top = jnp.max(top, axis=-1, keepdims=True)
-        return [jnp.exp2(p - top).astype(jnp.bfloat16) for p in pieces]
-
-    def settle(j, e, both):
-        at = pl.ds(pl.multiple_of(j * Q_BLOCK, Q_BLOCK), Q_BLOCK)
-        both = jnp.where(low_lanes(both.shape), jnp.ones_like(both), both)
-        o = jnp.dot(jnp.concatenate(e, axis=1), both, preferred_element_type=jnp.float32)
-        o = merge(o * pltpu.roll(1.0 / o, HEAD_DIM, 1), Q_BLOCK)
-        g = pltpu.roll(pltpu_pad(gate[at]), LANES - 2 * rank, 1)
-        mix[at] = (oc[at] + o * gate_lanes(g, 16, o.shape)).astype(jnp.bfloat16)
+        for a in range(EARLY_PICKS):
+            parts.append(got[near_sm[a, me * q_blocks + j] % OWNERS, j])
+        return jnp.concatenate(parts, axis=0)
+
+    def last_blocks(j):
+        parts = []
+        for a in range(EARLY_PICKS, FAR_PICKS):
+            mark = near_sm[a, me * q_blocks + j]
+            slow = (mark >= 32) & (mark < 64)
+            quick_block = got[jnp.where(slow, me, mark % OWNERS), j]
+            slow_block = late[jnp.where(slow, mark - 32, 0), j]
+            parts.append(jnp.where(slow, slow_block, quick_block))
+        return jnp.concatenate(parts, axis=0)
+
+    def biased(s, j, first):
+        return [
+            s[:, c : c + LANES]
+            + jnp.where(low_lane, bias_of(first + c // SEL_BLOCK, j), bias_of(first + c // SEL_BLOCK + 1, j))
+            for c in range(0, s.shape[1], LANES)
+        ]
+
+    def start_choice(i, carry):
+        js = [i * 2 + u for u in range(2)]
+        boths = [first_blocks(j) for j in js]
+        scores = [nt_dot(queries(j), both) for j, both in zip(js, boths)]
+        done = []
+        for j, s in zip(js, scores):
+            pieces = [jnp.where(later, MASKED, s[:, :Q_BLOCK])] + biased(s[:, Q_BLOCK:], j, 0)
+            top = jnp.max(functools.reduce(jnp.maximum, pieces), axis=-1, keepdims=True)
+            done.append((top, jnp.concatenate([jnp.exp2(p - top).astype(jnp.bfloat16) for p in pieces], axis=1)))
+        for j, (top, e), both in zip(js, done, boths):
+            first_out[j] = jnp.dot(e, with_ones(both), preferred_element_type=jnp.float32)
+            first_top[j] = jnp.broadcast_to(top, (2 * Q_BLOCK, LANES))
+        return carry
+
+    arrive(False)
+    lax.fori_loop(0, q_blocks // 2, start_choice, 0)
+    arrive(True)
 
     def choose(step, carry):
-        target = (rank + 1 + step) % RANKS
+        pl.when(step > 0)(lambda: mix_copy(step - 1).start())
+        target = mix_target(step)
         js = [target * group + u for u in range(group)]
-        scored = [score(j) for j in js]
-        es = [weights(s, biases) for s, _, biases in scored]
-        for j, e, (_, both, _) in zip(js, es, scored):
-            settle(j, e, both)
-        pl.when(step > 0)(lambda: mix_copy(step - 1).start())
+        boths = [last_blocks(j) for j in js]
+        scores = [nt_dot(queries(j), both) for j, both in zip(js, boths)]
+        done = []
+        for j, s in zip(js, scores):
+            pieces = biased(s, j, EARLY_PICKS)
+            old = first_top[j]
+            top = jnp.max(functools.reduce(jnp.maximum, pieces), axis=-1, keepdims=True)
+            top = jnp.maximum(old, top)
+            e = jnp.concatenate([jnp.exp2(p - top).astype(jnp.bfloat16) for p in pieces], axis=1)
+            done.append((e, jnp.exp2(old - top)))
+        for j, (e, keep), both in zip(js, done, boths):
+            at = pl.ds(pl.multiple_of(j * Q_BLOCK, Q_BLOCK), Q_BLOCK)
+            o = first_out[j] * keep + jnp.dot(e, with_ones(both), preferred_element_type=jnp.float32)
+            o = merge(o * pltpu.roll(1.0 / o, HEAD_DIM, 1), Q_BLOCK)
+            g = pltpu.roll(pltpu_pad(gate[at]), LANES - 2 * rank, 1)
+            mix[at] = (oc[at] + o * gate_lanes(g, 16, o.shape)).astype(jnp.bfloat16)
         return carry
 
     lax.fori_loop(0, RANKS, choose, 0)
@@ -488,8 +551,9 @@
         copy, _, _, sends, _ = hop(n)
         pl.when(sends)(copy.wait_send)
     for n in range(4):
-        copy, sends = span_copy(n)
-        pl.when(sends)(copy.wait_send)
+        for c in range(tiles):
+            copy, sends = span_copy(n, c)
+            pl.when(sends)(copy.wait_send)
     copies[9].wait()
     for step in range(RANKS - 1):
         mix_copy(step).wait_send()
@@ -588,6 +652,9 @@
             pltpu.VMEM((span, SEL_BLOCK, LANES), bf16),
             pltpu.VMEM((len(HOPS), q_blocks, SEL_BLOCK, LANES), bf16),
             pltpu.VMEM((OWNERS, q_blocks, SEL_BLOCK, LANES), bf16),
+            pltpu.VMEM((len(LATE), q_blocks, SEL_BLOCK, LANES), bf16),
+            pltpu.VMEM((q_blocks, 2 * Q_BLOCK, LANES), f32),
+            pltpu.VMEM((q_blocks, 2 * Q_BLOCK, LANES), f32),
             pltpu.VMEM((2, rows, LANES), bf16),
             pltpu.VMEM((2, rows, LANES), bf16),
             pltpu.VMEM((rows, LANES), f32),
@@ -604,8 +671,8 @@
             pltpu.SMEM((FAR_PICKS, picks), jnp.int32),
             dma((rows // 512,)),
             dma((12,)),
-            dma((4,)),
-            dma((2,)),
+            dma((4, 4)),
+            dma((2, 4)),
             dma((len(HOPS),)),
             dma((len(HOPS),)),
             dma((moves,)),

time: 65.3 us -> 63.7 us (0.975)
  the two profiles are of different devices: /device:TPU:73 before, /device:TPU:96 now
where the time goes in v5:
time: 63.7 us; the launch traced here: 63.5 us
  Pallas kernels  62.5 us (98%)
  local copies, waits for them, and re-layouts  0.97 us (2%)
    pallas_call x1, Pallas kernels, per_device(): pl.pallas_call(layer_kernel, in_specs=[vmem] * 7 + [hbm] * 11, out_specs=...  62.5 us

profile of v5, /device:TPU:96, one launch (start us, length us, event | category | flops | bytes accessed | tf_op | source)
XLA Modules:
  0.0 63.5 jit_solution(4159810113156854865)
XLA Ops:
  0.0 62.5 %layer.1 = bf16[256,2048]{1,0:T(8,128)(2,1)S(1)} custom-call(s32[8,256]{1,0:T(8,128)} %bitcast.29, bf16[2048]{0:T(1024)(128)(2,1)} %gain_ref.1, bf16[32,64]{1,0:T(8,128)(2,1)} %bitcast.30, bf16[64,64]{1,0:T(8,128)(2,1)} %bitcast.27, bf16[32,64]{1,0:T(8,128)(2,1)} %bitcast.31, bf16[64,64]{1,0:T(8,128)(2,1)} %bitcast.28, f32[128,128]{1,0:T(8,128)} %constant.4.clone.lo_ref, ...), custom_call_target="tpu_custom_call" | custom-call | flops 40000000000 | bytes 20000000 | tf_op jit(solution)/shard_map/layer/pallas_call | solution.py:636
  62.5 1.0 %copy.20 = bf16[256,2048]{1,0:T(8,128)(2,1)} copy(bf16[256,2048]{1,0:T(8,128)(2,1)S(1)} %layer.1) | data formatting | bytes 2097152

commit v6 on v4

--- a/solution.py
+++ b/solution.py
@@ -27,7 +27,11 @@
 
 MOVES = [(dz, dx) for dx in (2, 1, 3, 0) for dz in (2, 1, 3, 0) if (dz, dx) != (0, 0)]
 OWN, NEAR, FAR, SKIP = range(4)
-HOPS = [(kind, dx) for kind in (OWN, NEAR, FAR) for dx in (2, 1, 3)] + [(SKIP, dx) for dx in (0, 1, 3, 2)]
+HALVES = 2
+HOPS = [(OWN, dx, half) for half in range(HALVES) for dx in (2, 1, 3)]
+for half in range(HALVES):
+    HOPS += [(SKIP, dx, half) for dx in (0, 1, 3, 2)]
+    HOPS += [(kind, dx, half) for kind in (NEAR, FAR) for dx in (2, 1, 3)]
 
 
 def nt_dot(a, b):
@@ -79,7 +83,8 @@
     near,
     far,
     stage,
-    got,
+    got_even,
+    got_odd,
     qp,
     qt,
     ckv,
@@ -93,7 +98,7 @@
     heard,
     pick_vm,
     pick_sm,
-    near_sm,
+    owner_sm,
     tok_sem,
     local_sem,
     span_send,
@@ -113,6 +118,7 @@
     q_blocks = rows // Q_BLOCK
     span = rows // SEL_BLOCK
     blocks = rows // CMP_BLOCK
+    got = (got_even, got_odd)
     scale = HEAD_DIM ** (-0.5) * math.log2(math.e)
 
     sums[...] = jnp.zeros_like(sums)
@@ -154,11 +160,12 @@
         inside = jnp.where(chosen // span == owner, chosen % span, 0)
         index = jnp.where(line == kind, jnp.sum(inside, axis=0, keepdims=True), index)
     pick_vm[0] = index
-    pick_vm[1] = chosen
+    at_block = lax.broadcasted_iota(jnp.int32, chosen.shape, 1) * (Q_BLOCK // SEL_BLOCK)
+    pick_vm[1] = jnp.where(chosen < at_block, chosen // span, 64 + me)
     to_smem = pltpu.make_async_copy(pick_vm.at[0], pick_sm, local_sem.at[len(loads)])
-    near_smem = pltpu.make_async_copy(pick_vm.at[1], near_sm, local_sem.at[len(loads) + 1])
+    owner_smem = pltpu.make_async_copy(pick_vm.at[1], owner_sm, local_sem.at[len(loads) + 1])
     to_smem.start()
-    near_smem.start()
+    owner_smem.start()
 
     for copy in copies[:7]:
         copy.wait()
@@ -217,14 +224,6 @@
                 ref[0, to] = jnp.where(low, q, rest).astype(jnp.bfloat16)
                 ref[1, to] = jnp.where(low, pltpu.roll(q, HEAD_DIM, 1), rest).astype(jnp.bfloat16)
 
-    for i in range(tiles):
-        tok_copies[i].wait()
-        project(i)
-
-    to_smem.wait()
-    near_smem.wait()
-    pl.semaphore_wait(barrier, OWNERS + RANKS - 2)
-
     def route(dz, dx):
         there = ((z + dz) % PLANES) * ACROSS + (x + dx) % ACROSS
         here = ((z - dz) % PLANES) * ACROSS + (x - dx) % ACROSS
@@ -232,27 +231,40 @@
             return there, x + dx < ACROSS, here, x >= dx
         return there, z + dz < PLANES, here, z >= dz
 
-    def span_copy(n):
+    def span_copy(n, c):
         step, sends, source, target = (
             (1, z < 3, held, near),
             (3, z == 1, held, near),
             (3, z == 0, held, far),
             (3, z == 3, far, far),
         )[n]
+        at = pl.ds(c * (span // tiles), span // tiles)
         return (
             pltpu.make_async_remote_copy(
-                src_ref=source,
-                dst_ref=target,
-                send_sem=span_send.at[n],
-                recv_sem=span_recv.at[n // 2],
+                src_ref=source.at[at],
+                dst_ref=target.at[at],
+                send_sem=span_send.at[n, c],
+                recv_sem=span_recv.at[n // 2, c],
                 device_id={"kv": lax.rem(me + step * ACROSS, OWNERS)},
                 device_id_type=MESH,
             ),
             sends,
         )
 
+    for i in range(tiles):
+        tok_copies[i].wait()
+        project(i)
+        if i == 0:
+            pl.semaphore_wait(barrier, OWNERS + RANKS - 2)
+        for n in range(3):
+            copy, sends = span_copy(n, i)
+            pl.when(sends)(copy.start)
+
+    to_smem.wait()
+    owner_smem.wait()
+
     def hop(n):
-        kind, dx = HOPS[n]
+        kind, dx, half = HOPS[n]
         column = lax.rem(x + dx, ACROSS)
         back = lax.rem(x + ACROSS - dx, ACROSS)
         if kind == OWN:
@@ -266,7 +278,7 @@
         there = (3 if kind == SKIP else z) * ACROSS + column
         copy = pltpu.make_async_remote_copy(
             src_ref=stage.at[n],
-            dst_ref=got.at[owner],
+            dst_ref=got[half].at[owner],
             send_sem=send_sem.at[n],
             recv_sem=recv_sem.at[n],
             device_id={"kv": there},
@@ -275,39 +287,47 @@
         return copy, there, source, sends, gets
 
     def gather(source, kind, target, first):
-        def one(j, carry):
-            target[j] = source[pick_sm[kind, first + j]]
+        def one(p, carry):
+            target[p] = source[pick_sm[kind, first + HALVES * p]]
             return carry
 
-        lax.fori_loop(0, q_blocks, one, 0)
-
-    def send_hops(*kinds):
-        for n, (kind, dx) in enumerate(HOPS):
-            if kind in kinds:
+        lax.fori_loop(0, q_blocks // HALVES, one, 0)
+
+    def gather_own(source, kind, owner):
+        for half in range(HALVES):
+            gather(source, kind, got[half].at[owner], me * q_blocks + half)
+
+    def send_hops(which, part):
+        for n, (kind, dx, half) in enumerate(HOPS):
+            if kind == which and half == part:
                 copy, there, source, sends, _ = hop(n)
 
                 def go(n=n, kind=kind, copy=copy, there=there, source=source):
-                    gather(source, NEAR if kind == SKIP else kind, stage.at[n], there * q_blocks)
+                    first = there * q_blocks + part
+                    gather(source, NEAR if kind == SKIP else kind, stage.at[n], first)
                     copy.start()
 
                 pl.when(sends)(go)
 
-    for n in range(3):
-        copy, sends = span_copy(n)
-        pl.when(sends)(copy.start)
-    send_hops(OWN)
+    for half in range(HALVES):
+        send_hops(OWN, half)
 
     weigh(raw, 128, 160, 256)
 
-    def project_more(i, carry):
-        at = pl.ds(pl.multiple_of(i * tile, tile), tile)
+    def project_more(i):
+        at = pl.ds(i * tile, tile)
         y = nt_dot(tok[at], wt[256:416])
         inv = scales[at]
         ckv[at] = (y[:, 0:LANES] * inv).astype(jnp.bfloat16).astype(jnp.float32)
         gate[at] = jax.nn.sigmoid(y[:, LANES : LANES + 32] * inv[:, 0:32])
-        return carry
-
-    lax.fori_loop(0, tiles, project_more, 0)
+
+    def hand_back(c):
+        span_copy(2, c)[0].wait_recv()
+        span_copy(3, c)[0].start()
+
+    for c in range(tiles):
+        project_more(c)
+        pl.when(z == 3)(functools.partial(hand_back, c))
     for copy in copies[7:9]:
         copy.wait()
 
@@ -348,26 +368,18 @@
     for n in range(len(MOVES)):
         copy, _, sends, _ = sum_copy(n, me)
         pl.when(sends)(copy.start)
-    gather(held, OWN, got.at[me], me * q_blocks)
-
-    def pass_near():
-        send_hops(NEAR)
-        gather(near, NEAR, got.at[near_owner], me * q_blocks)
-
-    def hand_back():
-        span_copy(2)[0].wait_recv()
-        span_copy(3)[0].start()
-
-    def pass_far():
-        pl.when(z == 2)(span_copy(2)[0].wait_recv)
-        send_hops(FAR)
-        gather(far, FAR, got.at[far_owner], me * q_blocks)
-
-    pl.when(z == 3)(hand_back)
-    span_copy(0)[0].wait_recv()
-    send_hops(SKIP)
-    pl.when(z >= 1)(pass_near)
-    pl.when(z == 3)(pass_far)
+    gather_own(held, OWN, me)
+    for c in range(tiles):
+        span_copy(0, c)[0].wait_recv()
+    for half in range(HALVES):
+        send_hops(SKIP, half)
+        send_hops(NEAR, half)
+        if half == 0:
+            for c in range(tiles):
+                pl.when(z == 2)(span_copy(2, c)[0].wait_recv)
+        send_hops(FAR, half)
+    pl.when(z >= 1)(lambda: gather_own(near, NEAR, near_owner))
+    pl.when(z >= 2)(lambda: gather_own(far, FAR, far_owner))
     for n in range(len(MOVES)):
         _, here, _, gets = sum_copy(n, me)
         copy, _, _, _ = sum_copy(n, here)
@@ -406,46 +418,41 @@
     def pltpu_pad(g):
         return jnp.concatenate([g, g, g, g], axis=1)
 
-    lax.fori_loop(0, 3, compress, 0)
-    pl.when(z == 2)(pass_far)
-    lax.fori_loop(3, rows // part, compress, 0)
+    lax.fori_loop(0, rows // part, compress, 0)
 
     rank_rows = rows // RANKS
     group = rank_rows // Q_BLOCK
 
-    def mix_copy(step):
-        target = (rank + 1 + step) % RANKS
-        at = pl.ds(pl.multiple_of(target * rank_rows, rank_rows), rank_rows)
+    def mix_target(step):
+        mask = RANKS - 1 - step
+        return sum((rank // w + mask // w) % 2 * w for w in (4, 2, 1))
+
+    def mix_copy(half, step):
+        target = mix_target(step)
+        at = pl.ds(pl.multiple_of(target * rank_rows + half * Q_BLOCK, Q_BLOCK), Q_BLOCK)
         return pltpu.make_async_remote_copy(
             src_ref=mix.at[at],
-            dst_ref=heard.at[rank],
-            send_sem=mix_send.at[step],
-            recv_sem=mix_recv.at[step],
+            dst_ref=heard.at[half, rank],
+            send_sem=mix_send.at[half, step],
+            recv_sem=mix_recv.at[half, step],
             device_id={"tp": target},
             device_id_type=MESH,
         )
-
-    for n in range(len(HOPS)):
-        copy, _, _, _, gets = hop(n)
-        pl.when(gets)(copy.wait_recv)
 
     own_row = lax.broadcasted_iota(jnp.int32, (2 * Q_BLOCK, Q_BLOCK), 0)
     own_row = jnp.where(own_row >= Q_BLOCK, own_row - Q_BLOCK, own_row)
     later = lax.broadcasted_iota(jnp.int32, own_row.shape, 1) > own_row
     low_lane = lax.broadcasted_iota(jnp.int32, (1, LANES), 1) < SEL_BLOCK
 
-    def score(j):
+    def score(j, half):
         at = pl.ds(pl.multiple_of(j * Q_BLOCK, Q_BLOCK), Q_BLOCK)
         own = j * (Q_BLOCK // SEL_BLOCK)
         parts = [held[own + b] for b in range(Q_BLOCK // SEL_BLOCK)]
-        first = me * span + own
         biases = []
         for a in range(FAR_PICKS):
-            pick = near_sm[a, me * q_blocks + j]
-            usable = pick < first
-            owner = jnp.where(usable, pick // span, me)
-            parts.append(got[owner, j])
-            biases.append(jnp.where(usable, 0.0, MASKED))
+            mark = owner_sm[a, me * q_blocks + j]
+            parts.append(got[half][mark % OWNERS, j // HALVES])
+            biases.append(jnp.where(mark < 64, 0.0, MASKED))
         both = jnp.concatenate(parts, axis=0)
         q = jnp.concatenate([qt[0, at], qt[1, at]], axis=0)
         return nt_dot(q, both), both, biases
@@ -455,32 +462,51 @@
         for a in range(0, FAR_PICKS, 2):
             c = Q_BLOCK + a * SEL_BLOCK
             pieces.append(s[:, c : c + LANES] + jnp.where(low_lane, biases[a], biases[a + 1]))
-        top = functools.reduce(jnp.maximum, pieces)
-        top = jnp.max(top, axis=-1, keepdims=True)
-        return [jnp.exp2(p - top).astype(jnp.bfloat16) for p in pieces]
+        top = jnp.max(functools.reduce(jnp.maximum, pieces), axis=-1, keepdims=True)
+        return jnp.concatenate([jnp.exp2(p - top).astype(jnp.bfloat16) for p in pieces], axis=1)
 
     def settle(j, e, both):
         at = pl.ds(pl.multiple_of(j * Q_BLOCK, Q_BLOCK), Q_BLOCK)
         both = jnp.where(low_lanes(both.shape), jnp.ones_like(both), both)
-        o = jnp.dot(jnp.concatenate(e, axis=1), both, preferred_element_type=jnp.float32)
+        o = jnp.dot(e, both, preferred_element_type=jnp.float32)
         o = merge(o * pltpu.roll(1.0 / o, HEAD_DIM, 1), Q_BLOCK)
         g = pltpu.roll(pltpu_pad(gate[at]), LANES - 2 * rank, 1)
         mix[at] = (oc[at] + o * gate_lanes(g, 16, o.shape)).astype(jnp.bfloat16)
 
-    def choose(step, carry):
-        target = (rank + 1 + step) % RANKS
-        js = [target * group + u for u in range(group)]
-        scored = [score(j) for j in js]
+    def choose(half, i, carry):
+        for step in (2 * i - 2, 2 * i - 1):
+            pl.when(i > 0)(lambda step=step: mix_copy(half, step).start())
+        js = [mix_target(2 * i + u) * group + half for u in range(2)]
+        scored = [score(j, half) for j in js]
         es = [weights(s, biases) for s, _, biases in scored]
         for j, e, (_, both, _) in zip(js, es, scored):
             settle(j, e, both)
-        pl.when(step > 0)(lambda: mix_copy(step - 1).start())
         return carry
 
-    lax.fori_loop(0, RANKS, choose, 0)
-
-    own_at = pl.ds(pl.multiple_of(rank * rank_rows, rank_rows), rank_rows)
-    heard[rank] = mix[own_at]
+    for half in range(HALVES):
+        for n, (_, _, part_of) in enumerate(HOPS):
+            if part_of == half:
+                copy, _, _, _, gets = hop(n)
+                pl.when(gets)(copy.wait_recv)
+        lax.fori_loop(0, RANKS // 2, functools.partial(choose, half), 0)
+        mix_copy(half, RANKS - 2).start()
+        own_at = pl.ds(pl.multiple_of(rank * rank_rows + half * Q_BLOCK, Q_BLOCK), Q_BLOCK)
+        heard[half, rank] = mix[own_at]
+
+    copies[9].wait()
+    for half in range(HALVES):
+        for step in range(RANKS - 1):
+            mix_copy(half, step).wait_recv()
+        lhs = jnp.concatenate([heard[half, t] for t in range(RANKS)], axis=1)
+
+        def finish(c, carry, half=half, lhs=lhs):
+            at = pl.ds(pl.multiple_of(c * 512, 512), 512)
+            y = jnp.dot(lhs, wo[:, at], preferred_element_type=jnp.float32)
+            out_ref[half * Q_BLOCK : (half + 1) * Q_BLOCK, at] = y.astype(jnp.bfloat16)
+            return carry
+
+        lax.fori_loop(0, width // 512, finish, 0)
+
     for n in range(len(MOVES)):
         copy, _, sends, _ = sum_copy(n, me)
         pl.when(sends)(copy.wait_send)
@@ -488,21 +514,12 @@
         copy, _, _, sends, _ = hop(n)
         pl.when(sends)(copy.wait_send)
     for n in range(4):
-        copy, sends = span_copy(n)
-        pl.when(sends)(copy.wait_send)
-    copies[9].wait()
-    for step in range(RANKS - 1):
-        mix_copy(step).wait_send()
-        mix_copy(step).wait_recv()
-
-    lhs = jnp.concatenate([heard[t] for t in range(RANKS)], axis=1)
-
-    def finish(c, carry):
-        at = pl.ds(pl.multiple_of(c * 512, 512), 512)
-        out_ref[:, at] = jnp.dot(lhs, wo[:, at], preferred_element_type=jnp.float32).astype(jnp.bfloat16)
-        return carry
-
-    lax.fori_loop(0, width // 512, finish, 0)
+        for c in range(tiles):
+            copy, sends = span_copy(n, c)
+            pl.when(sends)(copy.wait_send)
+    for half in range(HALVES):
+        for step in range(RANKS - 1):
+            mix_copy(half, step).wait_send()
 
 
 def rope_tables(length):
@@ -586,8 +603,9 @@
             pltpu.VMEM((span, SEL_BLOCK, LANES), bf16),
             pltpu.VMEM((span, SEL_BLOCK, LANES), bf16),
             pltpu.VMEM((span, SEL_BLOCK, LANES), bf16),
-            pltpu.VMEM((len(HOPS), q_blocks, SEL_BLOCK, LANES), bf16),
-            pltpu.VMEM((OWNERS, q_blocks, SEL_BLOCK, LANES), bf16),
+            pltpu.VMEM((len(HOPS), q_blocks // HALVES, SEL_BLOCK, LANES), bf16),
+            pltpu.VMEM((OWNERS, q_blocks // HALVES, SEL_BLOCK, LANES), bf16),
+            pltpu.VMEM((OWNERS, q_blocks // HALVES, SEL_BLOCK, LANES), bf16),
             pltpu.VMEM((2, rows, LANES), bf16),
             pltpu.VMEM((2, rows, LANES), bf16),
             pltpu.VMEM((rows, LANES), f32),
@@ -598,20 +616,20 @@
             pltpu.VMEM((OWNERS * blocks, LANES), bf16),
             pltpu.VMEM((rows, LANES), f32),
             pltpu.VMEM((rows, LANES), bf16),
-            pltpu.VMEM((RANKS, rank_rows, LANES), bf16),
+            pltpu.VMEM((HALVES, RANKS, Q_BLOCK, LANES), bf16),
             pltpu.VMEM((2, FAR_PICKS, picks), jnp.int32),
             pltpu.SMEM((FAR_PICKS, picks), jnp.int32),
             pltpu.SMEM((FAR_PICKS, picks), jnp.int32),
             dma((rows // 512,)),
             dma((12,)),
-            dma((4,)),
-            dma((2,)),
+            dma((4, 4)),
+            dma((2, 4)),
             dma((len(HOPS),)),
             dma((len(HOPS),)),
             dma((moves,)),
             dma((moves,)),
-            dma((RANKS,)),
-            dma((RANKS,)),
+            dma((HALVES, RANKS)),
+            dma((HALVES, RANKS)),
         ],
         compiler_params=pltpu.CompilerParams(
             collective_id=0, has_side_effects=True, vmem_limit_bytes=60 * 1024 * 1024

time: 65.3 us -> 62.4 us (0.956)
  the two profiles are of different devices: /device:TPU:73 before, /device:TPU:96 now
where the time goes in v6:
time: 62.4 us; the launch traced here: 62.3 us
  Pallas kernels  61.3 us (98%)
  local copies, waits for them, and re-layouts  0.97 us (2%)
    pallas_call x1, Pallas kernels, per_device(): pl.pallas_call(layer_kernel, in_specs=[vmem] * 7 + [hbm] * 11, out_specs=...  61.3 us

profile of v6, /device:TPU:96, one launch (start us, length us, event | category | flops | bytes accessed | tf_op | source)
XLA Modules:
  0.0 62.3 jit_solution(17865232590096551106)
XLA Ops:
  0.0 61.3 %layer.1 = bf16[256,2048]{1,0:T(8,128)(2,1)S(1)} custom-call(s32[8,256]{1,0:T(8,128)} %bitcast.29, bf16[2048]{0:T(1024)(128)(2,1)} %gain_ref.1, bf16[32,64]{1,0:T(8,128)(2,1)} %bitcast.30, bf16[64,64]{1,0:T(8,128)(2,1)} %bitcast.27, bf16[32,64]{1,0:T(8,128)(2,1)} %bitcast.31, bf16[64,64]{1,0:T(8,128)(2,1)} %bitcast.28, f32[128,128]{1,0:T(8,128)} %constant.4.clone.lo_ref, ...), custom_call_target="tpu_custom_call" | custom-call | flops 40000000000 | bytes 20000000 | tf_op jit(solution)/shard_map/layer/pallas_call | solution.py:589
  61.3 1.0 %copy.20 = bf16[256,2048]{1,0:T(8,128)(2,1)} copy(bf16[256,2048]{1,0:T(8,128)(2,1)S(1)} %layer.1) | data formatting | bytes 2097152

commit v7 on v6

--- a/solution.py
+++ b/solution.py
@@ -274,7 +274,7 @@
         elif kind == FAR:
             owner, source, sends, gets = far_owner, far, z >= 2, z >= 2
         else:
-            owner, source, sends, gets = near_owner, near, z == 0, z == 3
+            owner, source, sends, gets = near_owner, near, z == (2 if dx == 0 else 0), z == 3
         there = (3 if kind == SKIP else z) * ACROSS + column
         copy = pltpu.make_async_remote_copy(
             src_ref=stage.at[n],
@@ -373,11 +373,12 @@
         span_copy(0, c)[0].wait_recv()
     for half in range(HALVES):
         send_hops(SKIP, half)
+        pl.when(z == 3)(functools.partial(send_hops, FAR, half))
         send_hops(NEAR, half)
         if half == 0:
             for c in range(tiles):
                 pl.when(z == 2)(span_copy(2, c)[0].wait_recv)
-        send_hops(FAR, half)
+        pl.when(z == 2)(functools.partial(send_hops, FAR, half))
     pl.when(z >= 1)(lambda: gather_own(near, NEAR, near_owner))
     pl.when(z >= 2)(lambda: gather_own(far, FAR, far_owner))
     for n in range(len(MOVES)):

time: 62.4 us -> 62.3 us (level)
  no operation moved by 1% of the time
where the time goes in v7:
time: 62.3 us; the launch traced here: 62.1 us
  Pallas kernels  61.1 us (98%)
  local copies, waits for them, and re-layouts  0.97 us (2%)
    pallas_call x1, Pallas kernels, per_device(): pl.pallas_call(layer_kernel, in_specs=[vmem] * 7 + [hbm] * 11, out_specs=...  61.1 us

profile of v7, /device:TPU:96, one launch (start us, length us, event | category | flops | bytes accessed | tf_op | source)
XLA Modules:
  0.0 62.1 jit_solution(2313578156719641763)
XLA Ops:
  0.0 61.1 %layer.1 = bf16[256,2048]{1,0:T(8,128)(2,1)S(1)} custom-call(s32[8,256]{1,0:T(8,128)} %bitcast.29, bf16[2048]{0:T(1024)(128)(2,1)} %gain_ref.1, bf16[32,64]{1,0:T(8,128)(2,1)} %bitcast.30, bf16[64,64]{1,0:T(8,128)(2,1)} %bitcast.27, bf16[32,64]{1,0:T(8,128)(2,1)} %bitcast.31, bf16[64,64]{1,0:T(8,128)(2,1)} %bitcast.28, f32[128,128]{1,0:T(8,128)} %constant.4.clone.lo_ref, ...), custom_call_target="tpu_custom_call" | custom-call | flops 40000000000 | bytes 20000000 | tf_op jit(solution)/shard_map/layer/pallas_call | solution.py:590
  61.2 1.0 %copy.20 = bf16[256,2048]{1,0:T(8,128)(2,1)} copy(bf16[256,2048]{1,0:T(8,128)(2,1)S(1)} %layer.1) | data formatting | bytes 2097152
